TPU v7x, 128 devices: a whole 4x4x4 slice. The times are simulated.
128 devices in a mesh: sp: 32 (over z, y, core), tp: 4 (over x).
Axes of the slice: x: 4, y: 4, z: 4, core: 2. Of those that a mesh axis runs over, the one named last changes fastest.
Arguments:
- queries: bfloat16 [16384, 1024], P('sp', 'tp'), may hold values from -260 to 260, as said below
- keys: bfloat16 [16384, 512], P('sp', 'tp'), may hold values from -8 to 8, as said below
- values: bfloat16 [16384, 512], P('sp', 'tp'), may hold values from -24 to 24
- doc_ids: int32 [16384], P('sp'), may hold values from 0 to 7, never falling along the last dimension, each value on 1 to 8192 neighbouring positions
- sink_logit: float32 [8], P('tp'), may hold values from 2 to 7
- residual_in: bfloat16 [16384, 2048], P(('sp', 'tp')), may hold values from -6 to 6
- w_out: bfloat16 [1024, 2048], replicated, may hold values from -0.375 to 0.375
- gain_one: float32 [2048], replicated, may hold values from 0.1 to 1.9
- w_gate: bfloat16 [2048, 5632], P('sp', 'tp'), may hold values from -0.125 to 0.125
- w_up: bfloat16 [2048, 5632], P('sp', 'tp'), may hold values from -0.125 to 0.125
- w_down: bfloat16 [5632, 2048], P('tp', 'sp'), may hold values from -0.078125 to 0.078125
- gain_two: float32 [2048], replicated, may hold values from 0.1 to 1.9
Outputs:
- layer_out: bfloat16 [16384, 2048], P(('sp', 'tp'))
Inputs may be any that keep to these rules, and one draw needn't show every extreme that they name: Real-valued projected queries. Real-valued projected keys. `doc_ids`: document numbers never fall along the sequence; each document is one run of positions.
All inputs are finite; a program needn't handle non-finite values.
Results may differ from a plain program's by a relative error of at most 0.012.
Values may be sent and summed in bfloat16 or wider, within the bound.
No kernel may reach another device: no remote copies, remote signals or barrier semaphores. Data moves between devices by JAX's collectives and lax.ppermute only.
A program may use at most 128 MiB of HBM per device.

v0:
```python
import math

import jax
import jax.numpy as jnp
from jax import lax
from jax.sharding import PartitionSpec as P

HEAD = 128
HALF = 128


ALPHA = 2.0**0.5
EPS = 1e-05
NEGATIVE = -1e30


def shifted(value, axis, steps):
    count = lax.axis_size(axis)
    leading, last = (max(0, -steps), min(count, count - steps))
    return lax.ppermute(value, axis, [(source, source + steps) for source in range(leading, last)])


def split_up(value, dim, devices):
    before, after = (value.shape[:dim], value.shape[dim + 1 :])
    return jnp.moveaxis(value.reshape(*before, devices, -1, *after), dim, 0)


def sum_at_owner(value, axis, dim):
    devices = lax.axis_size(axis)
    tiles = lax.all_to_all(split_up(value, dim, devices), axis, 0, 0, tiled=True)
    return jnp.sum(tiles.astype(jnp.float32), axis=0)


def laid_out(tiles, dim):
    lengths = list(tiles.shape[1:])
    lengths[dim] *= tiles.shape[0]
    return jnp.moveaxis(tiles, 0, dim).reshape(lengths)


def sent_to_all(value, axis):
    copies = jnp.broadcast_to(value, (lax.axis_size(axis), *value.shape))
    return lax.all_to_all(copies, axis, split_axis=0, concat_axis=0, tiled=True)


def gather_directly(value, axis, dim):
    return laid_out(sent_to_all(value, axis), dim)


def in_one_piece(arrays, axis, dim, along):
    ends, at = ([], 0)
    for a in arrays[:-1]:
        at += a.shape[along]
        ends.append(at)
    both = jnp.concatenate(arrays, axis=along)
    return tuple(jnp.split(lax.all_gather(both, axis, axis=dim, tiled=True), ends, axis=along))


def layer_norm(values_in, gain):
    average = jnp.mean(values_in, -1, keepdims=True)
    centred = values_in - average
    variance = jnp.mean(centred * centred, -1, keepdims=True)
    return centred * lax.rsqrt(variance + EPS) * gain


def per_device(
    queries,
    keys,
    values,
    doc_ids,
    sink_logit,
    residual_in,
    w_out,
    gain_one,
    w_gate,
    w_up,
    w_down,
    gain_two,
):
    row_count = queries.shape[0]
    sp_size = lax.axis_size("sp")
    kv_local = keys.shape[1] // HEAD
    repeat = queries.shape[1] // keys.shape[1]
    lower = (keys[row_count - HALF :], values[row_count - HALF :], doc_ids[row_count - HALF :])
    upper = (keys[:HALF], values[:HALF], doc_ids[:HALF])
    before = shifted((lower[0], lower[1], lower[2]), "sp", 1)
    after = shifted((upper[0], upper[1], upper[2]), "sp", -1)
    keys_all = jnp.concatenate([before[0], keys, after[0]], 0)
    values_all = jnp.concatenate([before[1], values, after[1]], 0)
    docs_all = jnp.concatenate([before[2], doc_ids, after[2]], 0)
    first_pos = lax.axis_index("sp") * row_count
    block = math.gcd(512, row_count)
    span = block + 2 * HALF
    sinks = sink_logit.reshape(kv_local, repeat)

    def one_block(index):
        start = index * block
        query_blk = queries.reshape(block, kv_local, repeat, HEAD)
        key_blk = keys_all.reshape(span, kv_local, HEAD)
        value_blk = values_all.reshape(span, kv_local, HEAD)
        pos_query = first_pos + start + jnp.arange(block, dtype=jnp.int32)
        pos_key = first_pos + start - HALF + jnp.arange(span, dtype=jnp.int32)
        offset = pos_key[None, :] - pos_query[:, None]
        allowed = (jnp.abs(offset) <= HALF) & (docs_all[None, :] == doc_ids[:, None])
        allowed = allowed & (pos_key[None, :] >= 0) & (pos_key[None, :] < sp_size * row_count)
        scores = jnp.einsum(
            "qgrd,kgd->grqk", query_blk, key_blk, preferred_element_type=jnp.float32
        ) * HEAD ** (-0.5)
        scores = jnp.where(allowed[None, None], scores, NEGATIVE)
        top = jnp.maximum(jnp.max(scores, -1), sinks[:, :, None])
        weights = jnp.exp(scores - top[..., None])
        total = jnp.sum(weights, -1) + jnp.exp(sinks[:, :, None] - top)
        summed = jnp.einsum(
            "grqk,kgd->qgrd",
            weights.astype(jnp.bfloat16),
            value_blk,
            preferred_element_type=jnp.float32,
        )
        scaled = summed / jnp.transpose(total, (2, 0, 1))[..., None]
        return scaled.reshape(block, kv_local * repeat * HEAD).astype(jnp.bfloat16)

    attended = lax.map(one_block, jnp.arange(row_count // block, dtype=jnp.int32)).reshape(
        row_count, -1
    )
    width = attended.shape[1]
    own_rows = lax.dynamic_slice_in_dim(w_out, lax.axis_index("tp") * width, width, 0)
    mixed_rows = sum_at_owner(
        jnp.dot(attended, own_rows, preferred_element_type=jnp.float32).astype(jnp.bfloat16),
        "tp",
        0,
    )
    pre_one = ALPHA * residual_in.astype(jnp.float32) + mixed_rows
    normed = layer_norm(pre_one, gain_one).astype(jnp.bfloat16)
    whole_rows = gather_directly(normed, "tp", 0)
    gate_whole, up_whole = in_one_piece((w_gate, w_up), "sp", 0, 1)
    gate_part = jnp.dot(whole_rows, gate_whole, preferred_element_type=jnp.float32)
    up_part = jnp.dot(whole_rows, up_whole, preferred_element_type=jnp.float32)
    hidden = (jax.nn.silu(gate_part) * up_part).astype(jnp.bfloat16)
    down_terms = jnp.dot(
        hidden, lax.all_gather(w_down, "sp", axis=1, tiled=True), preferred_element_type=jnp.float32
    )
    rounded = lax.optimization_barrier(down_terms.astype(jnp.bfloat16)).astype(jnp.float32)
    down_rows = sum_at_owner(rounded.astype(jnp.bfloat16), "tp", 0)
    pre_two = ALPHA * normed.astype(jnp.float32) + down_rows
    return layer_norm(pre_two, gain_two).astype(jnp.bfloat16)


def solution(mesh):
    in_specs = (
        P("sp", "tp"),
        P("sp", "tp"),
        P("sp", "tp"),
        P("sp"),
        P("tp"),
        P(("sp", "tp"), None),
        P(),
        P(),
        P("sp", "tp"),
        P("sp", "tp"),
        P("tp", "sp"),
        P(),
    )
    out_specs = P(("sp", "tp"), None)
    return jax.shard_map(
        per_device, mesh=mesh, in_specs=in_specs, out_specs=out_specs, check_vma=False
    )
```

profile of v0, /device:TPU:0, one launch (start us, length us, event | category | flops | bytes accessed | tf_op | source)
XLA Modules:
  0.0 175.9 jit_solution(14779466636091817606)
XLA Ops:
  6.5 1.8 %pad_maximum_fusion = bf16[64,2816]{1,0:T(8,128)(2,1)} fusion(bf16[64,1408]{1,0:T(8,128)(2,1)} %param.21, bf16[64,1408]{1,0:T(8,128)(2,1)} %param.20), kind=kLoop, calls=%fused_computation.32 | loop fusion | flops 720896 | bytes 720896 | tf_op jit(solution)/shard_map/concatenate | solution.py:54
  8.4 0.7 all-gather.5.cloned.1.call-update
  9.1 0.8 fusion.59
  9.9 1.3 collective-permute-start.2
  11.2 1.3 collective-permute-start.3
  12.5 0.8 fusion.58
  13.3 4.9 %collective-permute-start.4 = (bf16[128,128]{1,0:T(8,128)(2,1)S(1)}, bf16[128,128]{1,0:T(8,128)(2,1)S(1)}, u32[]{:S(2)}, u32[]{:S(2)}) collective-permute-start(bf16[128,128]{1,0:T(8,128)(2,1)S(1)} %get-tuple-element.23), channel_id=1, source_target_pairs={{0,4},{4,8},{8,12},{12,16},{16,20},{20,24},{24,28},{28,32},{32,36}... | collective-permute-start | bytes 98312 | tf_op jit(solution)/shard_map/ppermute | solution.py:20
  18.2 1.3 collective-permute-start.5
  19.5 1.0 copy.13
  20.5 4.3 %collective-permute-start = (bf16[128,128]{0,1:T(8,128)(2,1)S(1)}, bf16[128,128]{0,1:T(8,128)(2,1)S(1)}, u32[]{:S(2)}, u32[]{:S(2)}) collective-permute-start(bf16[128,128]{0,1:T(8,128)(2,1)S(1)} %get-tuple-element.21), channel_id=1, source_target_pairs={{0,4},{4,8},{8,12},{12,16},{16,20},{20,24},{24,28},{28,32},{32,36}... | collective-permute-start | bytes 98312 | tf_op jit(solution)/shard_map/ppermute | solution.py:20
  24.9 1.3 collective-permute-start.1
  26.2 0.7 pad_add_fusion
  26.9 1.6 fusion.18
  28.5 1.7 fusion.12
  30.3 0.7 fusion.10
  31.1 1.1 fusion.29
  32.2 2.0 %convolution_convert_fusion = bf16[512,2048]{1,0:T(8,128)(2,1)S(1)} fusion(bf16[512,256]{0,1:T(8,128)(2,1)S(1)} %bitcast.81, bf16[1024,2048]{1,0:T(8,128)(2,1)} %param.18, s32[]{:T(128)S(6)} %select_n.9), kind=kOutput, calls=%fused_computation.9 | convolution fusion | flops 537919488 | bytes 3407876 | tf_op jit(solution)/shard_map/dot_general | solution.py:127
  34.2 30.9 %all_to_all.15 = bf16[4,128,2048]{2,1,0:T(8,128)(2,1)S(1)} all-to-all(bf16[4,128,2048]{2,1,0:T(8,128)(2,1)S(1)} %bitcast.77), channel_id=1, replica_groups=mesh['sp'=32,'tp'=4] {'tp'}, dimensions={0} | all-to-all | bytes 4194304 | tf_op jit(solution)/shard_map/all_to_all | solution.py:30
  66.5 30.2 %all_to_all.16 = bf16[4,128,2048]{2,1,0:T(8,128)(2,1)S(1)} all-to-all(bf16[4,128,2048]{2,1,0:T(8,128)(2,1)S(1)} %broadcast_in_dim.47), channel_id=1, replica_groups=mesh['sp'=32,'tp'=4] {'tp'}, dimensions={0} | all-to-all | bytes 4194304 | tf_op jit(solution)/shard_map/all_to_all | solution.py:42
  96.7 7.6 %fusion.2 = f32[512,1408]{1,0:T(8,128)} fusion(bf16[512,2048]{1,0:T(8,128)(2,1)S(1)} %bitcast.78, bf16[2048,2816]{1,0:T(8,128)(2,1)} %all-gather.3.cloned.1.call-done), kind=kOutput, calls=%fused_computation.2 | convolution fusion | flops 2952790016 | bytes 10747904 | tf_op jit(solution)/shard_map/dot_general | solution.py:135
  104.3 18.4 %all-gather.5.cloned.1.call-done = bf16[1408,2048]{0,1:T(8,128)(2,1)} async-done(((bf16[1408,64]{0,1:T(8,128)(2,1)}), bf16[1408,2048]{0,1:T(8,128)(2,1)}) %all-gather.5.cloned.1.call-update) | async-done | bytes 5767184 | tf_op jit(solution)/shard_map/all_gather | solution.py:139
  122.7 13.3 %convolution_convert_fusion.1 = bf16[512,2048]{1,0:T(8,128)(2,1)} fusion(bf16[1408,2048]{0,1:T(8,128)(2,1)} %all-gather.5.cloned.1.call-done, bf16[512,2048]{1,0:T(8,128)(2,1)S(1)} %bitcast.79, bf16[2048,2816]{1,0:T(8,128)(2,1)} %all-gather.3.cloned.1.call-done, f32[512,1408]{1,0:T(8,128)} %fusion.2), kind=kOutput, calls=%fused_computation.11 | convolution fusion | flops 5910953984 | bytes 18612224 | tf_op jit(solution)/shard_map/dot_general | solution.py:138
  136.0 31.0 %all_to_all.17 = bf16[4,128,2048]{2,1,0:T(8,128)(2,1)S(1)} all-to-all(bf16[4,128,2048]{2,1,0:T(8,128)(2,1)} %bitcast.80), channel_id=1, replica_groups=mesh['sp'=32,'tp'=4] {'tp'}, dimensions={0} | all-to-all | bytes 4194304 | tf_op jit(solution)/shard_map/all_to_all | solution.py:30
  168.0 1.1 multiply_convert_fusion
  (38 shorter events, 2.7 us)
Async XLA Ops:
  6.5 22.0 %copy-start = (bf16[512,256]{1,0:T(8,128)(2,1)S(1)}, bf16[512,256]{1,0:T(8,128)(2,1)}, u32[]{:S(2)}) copy-start(bf16[512,256]{1,0:T(8,128)(2,1)} %param.12) | copy-start | bytes 786436
  6.5 90.2 %all-gather.3.cloned.1.call-start = ((), (), s32[]{:S(2)}) async-start(), calls=%async_computation.3 | async-start | bytes 11894784 | tf_op jit(solution)/shard_map/all_gather | solution.py:55
  8.4 21.8 %copy-start.4 = (f32[2]{0:T(128)S(1)}, f32[2]{0:T(128)}, u32[]{:S(2)}) copy-start(f32[2]{0:T(128)} %param.16) | copy-start | bytes 28
  8.4 114.4 %all-gather.5.cloned.1.call-start = ((), (), s32[]{:S(2)}) async-start(), calls=%async_computation.4 | async-start | bytes 5947392 | tf_op jit(solution)/shard_map/all_gather | solution.py:139
  9.9 15.0 %collective-permute-start.2 = (s32[128]{0:T(128)S(1)}, s32[128]{0:T(128)S(1)}, u32[]{:S(2)}, u32[]{:S(2)}) collective-permute-start(s32[128]{0:T(128)S(1)} %get-tuple-element.25), channel_id=1, source_target_pairs={{0,4},{4,8},{8,12},{12,16},{16,20},{20,24},{24,28},{28,32},{32,36}... | collective-permute-start | bytes 1544 | tf_op jit(solution)/shard_map/ppermute | solution.py:20
  11.2 15.0 %collective-permute-start.3 = (s32[128]{0:T(128)S(1)}, s32[128]{0:T(128)S(1)}, u32[]{:S(2)}, u32[]{:S(2)}) collective-permute-start(s32[128]{0:T(128)S(1)} %get-tuple-element.26), channel_id=1, source_target_pairs={{4,0},{8,4},{12,8},{16,12},{20,16},{24,20},{28,24},{32,28},{36,32}... | collective-permute-start | bytes 1544 | tf_op jit(solution)/shard_map/ppermute | solution.py:20
  13.3 15.2 %collective-permute-start.4 = (bf16[128,128]{1,0:T(8,128)(2,1)S(1)}, bf16[128,128]{1,0:T(8,128)(2,1)S(1)}, u32[]{:S(2)}, u32[]{:S(2)}) collective-permute-start(bf16[128,128]{1,0:T(8,128)(2,1)S(1)} %get-tuple-element.23), channel_id=1, source_target_pairs={{0,4},{4,8},{8,12},{12,16},{16,20},{20,24},{24,28},{28,32},{32,36}... | collective-permute-start | bytes 98312 | tf_op jit(solution)/shard_map/ppermute | solution.py:20
  18.2 10.3 %collective-permute-start.5 = (bf16[128,128]{1,0:T(8,128)(2,1)S(1)}, bf16[128,128]{1,0:T(8,128)(2,1)S(1)}, u32[]{:S(2)}, u32[]{:S(2)}) collective-permute-start(bf16[128,128]{1,0:T(8,128)(2,1)S(1)} %get-tuple-element.24), channel_id=1, source_target_pairs={{4,0},{8,4},{12,8},{16,12},{20,16},{24,20},{28,24},{32,28},{36,32}... | collective-permute-start | bytes 98312 | tf_op jit(solution)/shard_map/ppermute | solution.py:20
  20.5 10.5 %collective-permute-start = (bf16[128,128]{0,1:T(8,128)(2,1)S(1)}, bf16[128,128]{0,1:T(8,128)(2,1)S(1)}, u32[]{:S(2)}, u32[]{:S(2)}) collective-permute-start(bf16[128,128]{0,1:T(8,128)(2,1)S(1)} %get-tuple-element.21), channel_id=1, source_target_pairs={{0,4},{4,8},{8,12},{12,16},{16,20},{20,24},{24,28},{28,32},{32,36}... | collective-permute-start | bytes 98312 | tf_op jit(solution)/shard_map/ppermute | solution.py:20
  24.9 6.2 %collective-permute-start.1 = (bf16[128,128]{0,1:T(8,128)(2,1)S(1)}, bf16[128,128]{0,1:T(8,128)(2,1)S(1)}, u32[]{:S(2)}, u32[]{:S(2)}) collective-permute-start(bf16[128,128]{0,1:T(8,128)(2,1)S(1)} %get-tuple-element.22), channel_id=1, source_target_pairs={{4,0},{8,4},{12,8},{16,12},{20,16},{24,20},{28,24},{32,28},{36,32}... | collective-permute-start | bytes 98312 | tf_op jit(solution)/shard_map/ppermute | solution.py:20
  34.1 31.3 %copy-start.1 = (bf16[128,2048]{1,0:T(8,128)(2,1)S(1)}, bf16[128,2048]{1,0:T(8,128)(2,1)}, u32[]{:S(2)}) copy-start(bf16[128,2048]{1,0:T(8,128)(2,1)} %param.17) | copy-start | bytes 1572868
  65.0 0.9 copy-start.2
  167.0 1.0 copy-start.3
Sparse Core Ops, SparseCore 0:
  9.6 63.0 all-gather.2
  75.0 47.7 all-gather.4
where the time goes:
time: 177 us; the launch traced here: 176 us
  blocking collectives  92.1 us (52%)
  matrix products  25.6 us (14%)
  waiting for transfers between devices  19.1 us (11%)
  starting transfers between devices  14.4 us (8%)
  between operations  13.6 us (8%)
  other arithmetic  8.19 us (5%)
  local copies, waits for them, and re-layouts  2.83 us (2%)
    all_to_all x2, blocking collectives, sum_at_owner(): lax.all_to_all(split_up(value, dim, devices), axis, 0, 0, tiled=True)  61.9 us
    all_to_all x1, blocking collectives, sent_to_all(): return lax.all_to_all(copies, axis, split_axis=0, concat_axis=0, tiled=True)  30.2 us
    all_gather x1, waiting for transfers between devices, per_device(): lax.all_gather(w_down, 'sp', axis=1, tiled=True)  18.4 us
    ppermute x6, starting transfers between devices, shifted(): lax.ppermute(value, axis, [(source, source + steps) for source in range(l...  14.4 us
    dot_general x1, matrix products, per_device(): jnp.dot(hidden, lax.all_gather(w_down, 'sp', axis=1, tiled=True), preferr...  13.3 us
    dot_general x1, matrix products, per_device(): jnp.dot(whole_rows, gate_whole, preferred_element_type=jnp.float32)  7.62 us
  transfers between devices with their start and end apart: 8, of which 1 were waited for; matrix products, arithmetic and copies ran while one was open for 11% of the time, Pallas kernels for 0%

commit v1 on v0

v1 whole, which is shorter than its diff:
```python
import jax
import jax.numpy as jnp
from jax import lax
from jax.experimental import pallas as pl
from jax.experimental.pallas import tpu as pltpu
from jax.sharding import PartitionSpec as P


HEAD = 128
HALF = 128
ALPHA = 2.0**0.5
EPS = 1e-05
NEGATIVE = -1e30
BF, F32 = jnp.bfloat16, jnp.float32

ROWS = 512
OWN = 128
D = 2048
FFH = 704
GU = 2 * FFH
DN = 768
ORDER = (0, 1, 3, 2)
SP_Y, SP_Z = 2, 8


def swap(value, axis, mask):
    count = lax.axis_size(axis)
    return lax.ppermute(value, axis, [(i, i ^ mask) for i in range(count)])


def ring(value, axis, low):
    return [value] + [swap(value, axis, low * m) for m in ORDER[1:]]


def call(body, outs, flops, bytes_accessed, args, scratch=(), vmem_mib=20):
    vmem = pl.BlockSpec(memory_space=pltpu.VMEM)
    return pl.pallas_call(
        body,
        out_shape=outs,
        in_specs=[vmem] * len(args),
        out_specs=jax.tree.map(lambda _: vmem, outs),
        scratch_shapes=list(scratch),
        compiler_params=pltpu.CompilerParams(vmem_limit_bytes=vmem_mib << 20),
        cost_estimate=pl.CostEstimate(
            flops=flops, bytes_accessed=bytes_accessed, transcendentals=0
        ),
    )(*args)


def shape(dims, dtype=BF):
    return jax.ShapeDtypeStruct(dims, dtype)


def pack_body(gate, up, down, keep, send):
    core = lax.axis_index("sp") % 2
    lane = lax.broadcasted_iota(jnp.int32, (64, GU), 1)
    low = lane < FFH
    g, u, d = (r[...].astype(F32) for r in (gate, up, down))
    gr, ur, dr = (pltpu.roll(v, FFH, 1) for v in (g, u, d))
    first = jnp.where(low, g, ur)
    second = jnp.where(low, gr, u)
    d0 = jnp.where(low, d, 0.0)[:, :DN]
    d1 = jnp.where(low, dr, 0.0)[:, :DN]
    zero = core == 0
    keep[:, :GU] = jnp.where(zero, first, second).astype(BF)
    keep[:, GU:] = jnp.where(zero, d0, d1).astype(BF)
    send[:, :GU] = jnp.where(zero, second, first).astype(BF)
    send[:, GU:] = jnp.where(zero, d1, d0).astype(BF)


def attend_body(q, k, v, docs, sinks, side, far, out, kv, drow):
    sp = lax.axis_index("sp")
    core = sp % 2
    zero = core == 0
    before = jnp.where(zero, far[...].astype(F32), side[...].astype(F32))
    after = jnp.where(zero, side[...].astype(F32), far[...].astype(F32))
    kv[0:HALF, :] = before[:HALF].astype(BF)
    kv[HALF : HALF + ROWS, :HEAD] = k[...]
    kv[HALF : HALF + ROWS, HEAD:] = v[...]
    kv[HALF + ROWS :, :] = after[:HALF].astype(BF)
    drow[:, 0:HALF] = jnp.where(sp == 0, -1.0, before[HALF:, :HALF])
    drow[:, HALF : HALF + ROWS] = jnp.broadcast_to(docs[...].astype(F32), (8, ROWS))
    drow[:, HALF + ROWS :] = jnp.where(
        sp == lax.axis_size("sp") - 1, -1.0, after[HALF:, :HALF]
    )
    span = 3 * HALF
    row = lax.broadcasted_iota(jnp.int32, (HALF, span), 0)
    col = lax.broadcasted_iota(jnp.int32, (HALF, span), 1)
    near = jnp.abs(col - HALF - row) <= HALF
    for b in range(ROWS // HALF):
        dq = jnp.broadcast_to(drow[0:1, HALF + b * HALF : 2 * HALF + b * HALF], (HALF, HALF)).T
        dk = drow[0:1, b * HALF : b * HALF + span]
        same = jnp.concatenate([dq, dq, dq], 1) == dk
        ok = near & same
        keys = kv[b * HALF : b * HALF + span, :HEAD]
        vals = kv[b * HALF : b * HALF + span, HEAD:]
        for h in range(2):
            rows = slice(b * HALF, (b + 1) * HALF)
            cols = slice(h * HEAD, (h + 1) * HEAD)
            s = lax.dot_general(
                q[rows, cols], keys, (((1,), (1,)), ((), ())), preferred_element_type=F32
            ) * HEAD ** (-0.5)
            s = jnp.where(ok, s, NEGATIVE)
            sink = sinks[0:1, h : h + 1]
            top = jnp.maximum(jnp.max(s, -1, keepdims=True), sink)
            w = jnp.exp(s - top)
            total = jnp.sum(w, -1, keepdims=True) + jnp.exp(sink - top)
            o = jnp.dot(w.astype(BF), vals, preferred_element_type=F32)
            out[rows, cols] = (o / total).astype(BF)


def normalised(value):
    average = jnp.mean(value, -1, keepdims=True)
    centred = value - average
    variance = jnp.mean(centred * centred, -1, keepdims=True)
    return centred * lax.rsqrt(variance + EPS)


def chip(rz, ry):
    sp = lax.axis_index("sp")
    y, z = (sp // SP_Y) % 4, sp // SP_Z
    return pl.multiple_of(((z ^ rz) * 4 + (y ^ ry)) * 128, 128)


def norm_body(a0, a1, a3, a2, w_out, r0, r1, r3, r2, gain, out, mixed, nat, rot):
    x = lax.axis_index("tp")
    atts, res = (a0, a1, a3, a2), (r0, r1, r3, r2)
    for n in range(0, D, 512):
        acc = None
        for mask, a in zip(ORDER, atts):
            w = w_out[pl.ds(pl.multiple_of((x ^ mask) * 256, 256), 256), n : n + 512]
            t = jnp.dot(a[...], w, preferred_element_type=F32)
            acc = t if acc is None else acc + t
        mixed[:, n : n + 512] = acc
    for mask, r in zip(ORDER, res):
        for s in range(0, OWN, 32):
            at = pl.ds(pl.multiple_of((x ^ mask) * OWN + s, 32), 32)
            v = mixed[at, :] + ALPHA * r[s : s + 32, :].astype(F32)
            n = normalised(v) * gain[...]
            nat[at, :] = n
    for t in range(0, D, 128):
        rot[:, t : t + 128] = pltpu.roll(nat[:, t : t + 128], 64, 1)
    low = lax.broadcasted_iota(jnp.int32, (ROWS, 128), 1) < 64
    for i in range(4):
        for j in (0, 2):
            a, b = (pl.ds(chip(ORDER[i], ORDER[k]), 128) for k in (j, j + 1))
            dst = (i * 4 + j) * 64
            out[:, dst : dst + 128] = jnp.where(low, nat[:, a], rot[:, b]).astype(BF)
            a, b = (pl.ds(chip(ORDER[k], ORDER[i]), 128) for k in (j, j + 1))
            dst += 1024
            out[:, dst : dst + 128] = jnp.where(low, rot[:, a], nat[:, b]).astype(BF)


def hidden_body(mine, other, *refs):
    pieces, out, acc = refs[:10], refs[10], refs[11]
    for half, src in enumerate((mine, other)):
        for n in range(0, GU, 256):
            m = min(n + 256, GU)
            w = jnp.concatenate([p[:, n:m] for p in pieces], 0)
            acc[:, n:m] = jnp.dot(src[...], w, preferred_element_type=F32)
        for s in range(0, ROWS, 64):
            v = acc[s : s + 64, :]
            up = pltpu.roll(v, FFH, 1)[:, :DN]
            gate = v[:, :DN]
            h = gate / (1.0 + jnp.exp(-gate)) * up
            live = lax.broadcasted_iota(jnp.int32, (64, DN), 1) < FFH
            out[half * ROWS + s : half * ROWS + s + 64, :] = jnp.where(live, h, 0.0).astype(BF)


def down_part(h, p):
    return lax.dot_general(h, p, (((1,), (1,)), ((), ())), preferred_element_type=F32)


def give_body(h, *refs):
    pieces, out = refs[:-1], refs[-1]
    at = 0
    for p in pieces:
        width = p.shape[0]
        out[:, at : at + width] = down_part(h[ROWS:, :], p[...]).astype(BF)
        at += width


def take_body(h, theirs, *refs):
    pieces, (s0, s1, s3, s2, own) = refs[:-5], refs[-5:]
    x = lax.axis_index("tp")
    at = 0
    for p in pieces:
        width = p.shape[0]
        cols = slice(at, at + width)
        own[:, cols] = down_part(h[:ROWS, :], p[...]) + theirs[:, cols].astype(F32)
        at += width
    for mask, dst in zip(ORDER, (s0, s1, s3, s2)):
        rows = pl.ds(pl.multiple_of((x ^ mask) * OWN, OWN), OWN)
        dst[...] = own[rows, :].astype(dst.dtype)


def final_body(normed, gain, *refs):
    parts, out, pre = refs[:12], refs[12], refs[13]
    x = lax.axis_index("tp")
    xs = pl.ds(pl.multiple_of(x * OWN, OWN), OWN)
    for c, (first, width) in enumerate(((0, 256), (256, 512), (768, 256))):
        s = [r for r in parts[4 * c : 4 * c + 4]]
        v = s[0][...] + s[1][...].astype(F32) + s[2][...].astype(F32) + s[3][...].astype(F32)
        for kind in range(2):
            dst = slice(kind * 1024 + first, kind * 1024 + first + width)
            n = normed[xs, dst].astype(F32)
            pre[:, dst] = ALPHA * n + v[:, kind * width : (kind + 1) * width]
    pre[...] = normalised(pre[...])
    low = lax.broadcasted_iota(jnp.int32, (OWN, 128), 1) < 64
    for i in range(4):
        for j in range(4):
            p, q = 4 * i + j, 4 * j + i
            a = pre[:, (p // 2) * 128 : (p // 2) * 128 + 128]
            b = pre[:, 1024 + (q // 2) * 128 : 1024 + (q // 2) * 128 + 128]
            if p % 2 == 1:
                a = pltpu.roll(a, 64, 1)
            if q % 2 == 0:
                b = pltpu.roll(b, 64, 1)
            at = pl.ds(chip(ORDER[i], ORDER[j]), 128)
            out[:, at] = (jnp.where(low, a, b) * gain[:, at]).astype(BF)


def spread(col, low):
    one = swap(col, "sp", low)
    three = swap(col, "sp", 3 * low)
    mid = col.shape[0] // 2
    two_a = swap(one[:mid], "sp", 3 * low)
    two_b = swap(three[mid:], "sp", low)
    return col, one, three, two_a, two_b


def per_device(
    queries,
    keys,
    values,
    doc_ids,
    sink_logit,
    residual_in,
    w_out,
    gain_one,
    w_gate,
    w_up,
    w_down,
    gain_two,
):
    core = lax.axis_index("sp") % 2
    keep, send = call(
        pack_body, (shape((64, GU + DN)),) * 2, 10**6, 10**6, (w_gate, w_up, w_down.T)
    )
    recv = swap(send, "sp", 1)
    from_0 = jnp.where(core == 0, keep, recv)
    from_1 = jnp.where(core == 0, recv, keep)

    docs8 = jnp.broadcast_to(doc_ids.astype(BF).reshape(1, ROWS), (8, ROWS))

    def edge(rows):
        kv = jnp.concatenate([keys[rows], values[rows]], 1)
        d = docs8[:, rows]
        return jnp.concatenate([kv, jnp.concatenate([d, d], 1)], 0)

    last, first = edge(slice(ROWS - HALF, ROWS)), edge(slice(0, HALF))
    side = swap(jnp.where(core == 0, last, first), "sp", 1)
    count = lax.axis_size("sp")
    pairs = [(i, i + 1) for i in range(1, count - 1, 2)]
    far = lax.ppermute(
        jnp.where(core == 0, first, last), "sp", pairs + [(b, a) for a, b in pairs]
    )

    res = ring(residual_in, "tp", 1)

    def columns(origin, near, across):
        units = ring(origin, "sp", near)
        gu = jnp.concatenate([u[:, :GU] for u in units], 0)
        dn = jnp.concatenate([u[:, GU:] for u in units], 0)
        return spread(gu, across), ring(dn, "sp", across)

    gu_a, dn_a = columns(from_0, SP_Y, SP_Z)
    gu_b, dn_b = columns(from_1, SP_Z, SP_Y)

    attended = call(
        attend_body,
        shape((ROWS, 256)),
        4 * ROWS * 256 * 384 * 8,
        10**6,
        (queries, keys, values, doc_ids.reshape(1, ROWS), sink_logit.reshape(1, 2), side, far),
        (pltpu.VMEM((ROWS + 2 * HALF, 256), BF), pltpu.VMEM((8, ROWS + 2 * HALF), F32)),
    )
    atts = ring(attended, "tp", 1)
    mine = call(
        norm_body,
        shape((ROWS, D)),
        2 * ROWS * 1024 * D * 2,
        10**7,
        (*atts, w_out, *res, gain_one.reshape(1, D)),
        (pltpu.VMEM((ROWS, D), F32),) * 3,
    )
    other = swap(mine, "sp", 1)
    hidden = call(
        hidden_body,
        shape((2 * ROWS, DN)),
        2 * 2 * ROWS * D * GU,
        10**7,
        (mine, other, *gu_a, *gu_b),
        (pltpu.VMEM((ROWS, GU), F32),),
    )
    sums = []
    chunks = [slice(0, 1), slice(1, 3), slice(3, 4)]
    for part_of in chunks:
        pieces = (*dn_a[part_of], *dn_b[part_of])
        width = sum(p.shape[0] for p in pieces)
        flops = 2 * ROWS * DN * width
        part = call(give_body, shape((ROWS, width)), flops, 10**6, (hidden, *pieces))
        theirs = swap(part, "sp", 1)
        s0, *rest = call(
            take_body,
            (shape((OWN, width), F32),) + (shape((OWN, width)),) * 3,
            flops,
            10**6,
            (hidden, theirs, *pieces),
            (pltpu.VMEM((ROWS, width), F32),),
        )
        sums += [s0] + [swap(r, "tp", m) for r, m in zip(rest, ORDER[1:])]
    return call(
        final_body,
        shape((OWN, D)),
        10**6,
        10**6,
        (mine, gain_two.reshape(1, D), *sums),
        (pltpu.VMEM((OWN, D), F32),),
    )


def solution(mesh):
    in_specs = (
        P("sp", "tp"),
        P("sp", "tp"),
        P("sp", "tp"),
        P("sp"),
        P("tp"),
        P(("sp", "tp"), None),
        P(),
        P(),
        P("sp", "tp"),
        P("sp", "tp"),
        P("tp", "sp"),
        P(),
    )
    out_specs = P(("sp", "tp"), None)
    return jax.shard_map(
        per_device, mesh=mesh, in_specs=in_specs, out_specs=out_specs, check_vma=False
    )
```

time: 177 us -> 180 us (1.017)
  blocking collectives: 92.1 us -> 0 us
  starting transfers between devices: 14.4 us -> 86 us
  waiting for transfers between devices: 19.1 us -> 63.7 us
  matrix products: 25.6 us -> 0 us
  Pallas kernels: 0 us -> 22.9 us
  between operations: 13.6 us -> 0.45 us
  other arithmetic: 8.19 us -> 0.95 us
  local copies, waits for them, and re-layouts: 2.83 us -> 5.26 us
    all_to_all x3 -> x0, blocking collectives: 92.1 us -> none  [the longest x2 61.9 us: sum_at_owner(): lax.all_to_all(split_up(value, dim, devices), axis, 0, 0, tiled=True)]
    ppermute x6 -> x42, starting transfers between devices: 14.4 us -> 86 us  [the longest x41 85.3 us: swap(): return lax.ppermute(value, axis, [(i, i ^ mask) for i in range(count)])]
    ppermute x6 -> x42, waiting for transfers between devices: 0.02 us -> 63.7 us  [the longest x41 63.7 us: swap(): return lax.ppermute(value, axis, [(i, i ^ mask) for i in range(count)])]
    dot_general x5 -> x0, matrix products: 25.6 us -> none  [the longest x1 13.3 us: per_device(): jnp.dot(hidden, lax.all_gather(w_down, 'sp', axis=1, tiled=True), preferr...]
    pallas_call x0 -> x11, Pallas kernels: none -> 22.9 us  [call(): pl.pallas_call(body, out_shape=outs, in_specs=[vmem] * len(args), out_spe...]
    all_gather x2 -> x0, waiting for transfers between devices: 18.4 us -> none  [the longest x1 18.4 us: per_device(): lax.all_gather(w_down, 'sp', axis=1, tiled=True)]
    unnamed x11 -> x24, local copies, waits for them, and re-layouts: 1.03 us -> 4.13 us
    reduce_sum x7 -> x0, other arithmetic: 2.58 us -> none  [the longest x2 0.76 us: sum_at_owner(): return jnp.sum(tiles.astype(jnp.float32), axis=0)]
  transfers between devices with their start and end apart: 8 -> 42, of which waited for: 1 -> 13; matrix products, arithmetic and copies ran while one was open for 11% -> 0% of each run, Pallas kernels for 0% -> 10%
where the time goes in v1:
time: 180 us; the launch traced here: 179 us
  starting transfers between devices  86 us (48%)
  waiting for transfers between devices  63.7 us (35%)
  Pallas kernels  22.9 us (13%)
  local copies, waits for them, and re-layouts  5.26 us (3%)
    ppermute x41, starting transfers between devices, swap(): return lax.ppermute(value, axis, [(i, i ^ mask) for i in range(count)])  85.3 us
    ppermute x41, waiting for transfers between devices, swap(): return lax.ppermute(value, axis, [(i, i ^ mask) for i in range(count)])  63.7 us
    pallas_call x11, Pallas kernels, call(): pl.pallas_call(body, out_shape=outs, in_specs=[vmem] * len(args), out_spe...  22.9 us
    unnamed x24, local copies, waits for them, and re-layouts  4.13 us
  transfers between devices with their start and end apart: 42, of which 13 were waited for; matrix products, arithmetic and copies ran while one was open for 0% of the time, Pallas kernels for 10%

profile of v1, /device:TPU:0, one launch (start us, length us, event | category | flops | bytes accessed | tf_op | source)
XLA Modules:
  0.0 179.2 jit_solution(11740142638531170818)
XLA Ops:
  7.1 2.9 %shard_map.118.a0 = bf16[512,256]{1,0:T(8,128)(2,1)S(1)} custom-call(bf16[512,256]{1,0:T(8,128)(2,1)S(1)} %copy-done.9, bf16[512,128]{1,0:T(8,128)(2,1)S(1)} %copy-done.3, bf16[512,128]{1,0:T(8,128)(2,1)S(1)} %copy-done.4, s32[1,512]{1,0:T(1,128)S(1)} %bitcast.7, f32[1,2]{1,0:T(1,128)S(1)} %bitcast.9, bf16[136,256]{1,0:T(8,128)(2,1)S(1)} %collective-permute-done.side, ...), custom_call_target="tpu_custom_call" | custom-call | flops 1610612736 | bytes 1000000 | tf_op jit(solution)/shard_map/pallas_call | solution.py:37
  12.1 2.9 %collective-permute-start.6 = (bf16[128,2048]{1,0:T(8,128)(2,1)S(1)}, bf16[128,2048]{1,0:T(8,128)(2,1)S(1)}, u32[]{:S(2)}, u32[]{:S(2)}) collective-permute-start(bf16[128,2048]{1,0:T(8,128)(2,1)S(1)} %copy-done.8), channel_id=1, source_target_pairs={{0,3},{1,2},{2,1},{3,0},{4,7},{5,6},{6,5},{7,4},{8,11},{9,10},{10,... | collective-permute-start | bytes 1572872 | tf_op jit(solution)/shard_map/ppermute | solution.py:28
  19.8 13.3 %collective-permute-done.3.a3 = bf16[512,256]{1,0:T(8,128)(2,1)S(1)} collective-permute-done((bf16[512,256]{1,0:T(8,128)(2,1)S(1)}, bf16[512,256]{1,0:T(8,128)(2,1)S(1)}, u32[]{:S(2)}, u32[]{:S(2)}) %collective-permute-start.3) | collective-permute-done | bytes 262176 | tf_op jit(solution)/shard_map/ppermute | solution.py:28
  33.1 17.3 %collective-permute-start.9 = (bf16[64,2176]{1,0:T(8,128)(2,1)S(1)}, bf16[64,2176]{1,0:T(8,128)(2,1)S(1)}, u32[]{:S(2)}, u32[]{:S(2)}) collective-permute-start(bf16[64,2176]{1,0:T(8,128)(2,1)S(1)} %get-tuple-element.20), channel_id=1, source_target_pairs={{0,4},{4,0},{8,12},{12,8},{16,20},{20,16},{24,28},{28,24},{32,36},... | collective-permute-start | bytes 835592 | tf_op jit(solution)/shard_map/ppermute | solution.py:28
  50.4 6.5 %shard_map.119.mine.normed = bf16[512,2048]{1,0:T(8,128)(2,1)S(1)} custom-call(bf16[512,256]{1,0:T(8,128)(2,1)S(1)} %shard_map.118.a0, bf16[512,256]{1,0:T(8,128)(2,1)S(1)} %collective-permute-done.2.a1, bf16[512,256]{1,0:T(8,128)(2,1)S(1)} %collective-permute-done.3.a3, bf16[512,256]{1,0:T(8,128)(2,1)S(1)} %collective-permute-done.4.a2, ...), custom_call_target="tpu_custom_call" | custom-call | flops 4294967296 | bytes 10000000 | tf_op jit(solution)/shard_map/pallas_call | solution.py:37
  57.2 5.8 %collective-permute-start.10 = (bf16[64,2176]{1,0:T(8,128)(2,1)S(1)}, bf16[64,2176]{1,0:T(8,128)(2,1)S(1)}, u32[]{:S(2)}, u32[]{:S(2)}) collective-permute-start(bf16[64,2176]{1,0:T(8,128)(2,1)S(1)} %get-tuple-element.34), channel_id=1, source_target_pairs={{0,8},{4,12},{8,0},{12,4},{16,24},{20,28},{24,16},{28,20},{32,40},... | collective-permute-start | bytes 835592 | tf_op jit(solution)/shard_map/ppermute | solution.py:28
  68.1 2.4 %collective-permute-done.10 = bf16[64,2176]{1,0:T(8,128)(2,1)S(1)} collective-permute-done((bf16[64,2176]{1,0:T(8,128)(2,1)S(1)}, bf16[64,2176]{1,0:T(8,128)(2,1)S(1)}, u32[]{:S(2)}, u32[]{:S(2)}) %collective-permute-start.10) | collective-permute-done | bytes 278560 | tf_op jit(solution)/shard_map/ppermute | solution.py:28
  70.5 4.4 %collective-permute-start.18 = (bf16[64,2176]{1,0:T(8,128)(2,1)S(1)}, bf16[64,2176]{1,0:T(8,128)(2,1)S(1)}, u32[]{:S(2)}, u32[]{:S(2)}) collective-permute-start(bf16[64,2176]{1,0:T(8,128)(2,1)S(1)} %get-tuple-element.33), channel_id=1, source_target_pairs={{0,96},{4,100},{8,104},{12,108},{16,112},{20,116},{24,120},{28,124... | collective-permute-start | bytes 835592 | tf_op jit(solution)/shard_map/ppermute | solution.py:28
  74.9 2.5 %collective-permute-done.11 = bf16[64,2176]{1,0:T(8,128)(2,1)S(1)} collective-permute-done((bf16[64,2176]{1,0:T(8,128)(2,1)S(1)}, bf16[64,2176]{1,0:T(8,128)(2,1)S(1)}, u32[]{:S(2)}, u32[]{:S(2)}) %collective-permute-start.11) | collective-permute-done | bytes 278560 | tf_op jit(solution)/shard_map/ppermute | solution.py:28
  77.4 3.9 %collective-permute-start.19 = (bf16[64,2176]{1,0:T(8,128)(2,1)S(1)}, bf16[64,2176]{1,0:T(8,128)(2,1)S(1)}, u32[]{:S(2)}, u32[]{:S(2)}) collective-permute-start(bf16[64,2176]{1,0:T(8,128)(2,1)S(1)} %get-tuple-element.33), channel_id=1, source_target_pairs={{0,64},{4,68},{8,72},{12,76},{16,80},{20,84},{24,88},{28,92},{32,9... | collective-permute-start | bytes 835592 | tf_op jit(solution)/shard_map/ppermute | solution.py:28
  81.4 2.2 %collective-permute-start.13 = (bf16[256,1408]{1,0:T(8,128)(2,1)S(1)}, bf16[256,1408]{1,0:T(8,128)(2,1)S(1)}, u32[]{:S(2)}, u32[]{:S(2)}) collective-permute-start(bf16[256,1408]{1,0:T(8,128)(2,1)S(1)} %pad_maximum_fusion.refs_0_), channel_id=1, source_target_pairs={{0,32},{4,36},{8,40},{12,44},{16,48},{20,52},{24,56},{28,60},{32,0... | collective-permute-start | bytes 2162696 | tf_op jit(solution)/shard_map/ppermute | solution.py:28
  83.8 4.9 %collective-permute-done.19 = bf16[64,2176]{1,0:T(8,128)(2,1)S(1)} collective-permute-done((bf16[64,2176]{1,0:T(8,128)(2,1)S(1)}, bf16[64,2176]{1,0:T(8,128)(2,1)S(1)}, u32[]{:S(2)}, u32[]{:S(2)}) %collective-permute-start.19) | collective-permute-done | bytes 278560 | tf_op jit(solution)/shard_map/ppermute | solution.py:28
  90.7 2.4 %collective-permute-start.21 = (bf16[256,1408]{1,0:T(8,128)(2,1)S(1)}, bf16[256,1408]{1,0:T(8,128)(2,1)S(1)}, u32[]{:S(2)}, u32[]{:S(2)}) collective-permute-start(bf16[256,1408]{1,0:T(8,128)(2,1)S(1)} %pad_maximum_fusion.1.refs_5_), channel_id=1, source_target_pairs={{0,24},{4,28},{8,16},{12,20},{16,8},{20,12},{24,0},{28,4},{32,56},... | collective-permute-start | bytes 2162696 | tf_op jit(solution)/shard_map/ppermute | solution.py:28
  93.1 9.5 %collective-permute-done.13.refs_1_ = bf16[256,1408]{1,0:T(8,128)(2,1)S(1)} collective-permute-done((bf16[256,1408]{1,0:T(8,128)(2,1)S(1)}, bf16[256,1408]{1,0:T(8,128)(2,1)S(1)}, u32[]{:S(2)}, u32[]{:S(2)}) %collective-permute-start.13) | collective-permute-done | bytes 720928 | tf_op jit(solution)/shard_map/ppermute | solution.py:28
  105.0 3.8 %collective-permute-start.22 = (bf16[128,1408]{1,0:T(8,128)(2,1)S(1)}, bf16[128,1408]{1,0:T(8,128)(2,1)S(1)}, u32[]{:S(2)}, u32[]{:S(2)}) collective-permute-start(bf16[128,1408]{1,0:T(8,128)(2,1)S(1)} %slice.117), channel_id=1, source_target_pairs={{0,24},{4,28},{8,16},{12,20},{16,8},{20,12},{24,0},{28,4},{32,56},... | collective-permute-start | bytes 1081352 | tf_op jit(solution)/shard_map/ppermute | solution.py:28
  109.1 3.2 %collective-permute-done.15.refs_3_ = bf16[128,1408]{1,0:T(8,128)(2,1)S(1)} collective-permute-done((bf16[128,1408]{1,0:T(8,128)(2,1)S(1)}, bf16[128,1408]{1,0:T(8,128)(2,1)S(1)}, u32[]{:S(2)}, u32[]{:S(2)}) %collective-permute-start.15) | collective-permute-done | bytes 360480 | tf_op jit(solution)/shard_map/ppermute | solution.py:28
  116.4 2.5 %collective-permute-start.29 = (bf16[256,768]{1,0:T(8,128)(2,1)S(1)}, bf16[256,768]{1,0:T(8,128)(2,1)S(1)}, u32[]{:S(2)}, u32[]{:S(2)}) collective-permute-start(bf16[256,768]{1,0:T(8,128)(2,1)S(1)} %pad_maximum_fusion.2.refs_0_), channel_id=1, source_target_pairs={{0,96},{4,100},{8,104},{12,108},{16,112},{20,116},{24,120},{28,124... | collective-permute-start | bytes 1179656 | tf_op jit(solution)/shard_map/ppermute | solution.py:28
  122.0 6.8 %shard_map.121.h = bf16[1024,768]{1,0:T(8,128)(2,1)S(1)} custom-call(bf16[512,2048]{1,0:T(8,128)(2,1)S(1)} %shard_map.119.mine.normed, bf16[512,2048]{1,0:T(8,128)(2,1)S(1)} %collective-permute-done.8.other, bf16[256,1408]{1,0:T(8,128)(2,1)S(1)} %pad_maximum_fusion.refs_0_, bf16[256,1408]{1,0:T(8,128)(2,1)S(1)} %collective-permute-done.13.refs_1_, ...), custom_call_target="tpu_custom_call" | custom-call | flops 5905580032 | bytes 10000000 | tf_op jit(solution)/shard_map/pallas_call | solution.py:37
  132.8 3.6 %collective-permute-start.37 = (bf16[256,768]{1,0:T(8,128)(2,1)S(1)}, bf16[256,768]{1,0:T(8,128)(2,1)S(1)}, u32[]{:S(2)}, u32[]{:S(2)}) collective-permute-start(bf16[256,768]{1,0:T(8,128)(2,1)S(1)} %pad_maximum_fusion.3.refs_1_), channel_id=1, source_target_pairs={{0,16},{4,20},{8,24},{12,28},{16,0},{20,4},{24,8},{28,12},{32,48},... | collective-permute-start | bytes 1179656 | tf_op jit(solution)/shard_map/ppermute | solution.py:28
  136.4 9.7 %collective-permute-done.37.refs_1_ = bf16[256,768]{1,0:T(8,128)(2,1)S(1)} collective-permute-done((bf16[256,768]{1,0:T(8,128)(2,1)S(1)}, bf16[256,768]{1,0:T(8,128)(2,1)S(1)}, u32[]{:S(2)}, u32[]{:S(2)}) %collective-permute-start.37) | collective-permute-done | bytes 393248 | tf_op jit(solution)/shard_map/ppermute | solution.py:28
  149.8 2.8 %collective-permute-start.40 = (bf16[128,512]{1,0:T(8,128)(2,1)S(1)}, bf16[128,512]{1,0:T(8,128)(2,1)S(1)}, u32[]{:S(2)}, u32[]{:S(2)}) collective-permute-start(bf16[128,512]{1,0:T(8,128)(2,1)S(1)} %get-tuple-element.31), channel_id=1, source_target_pairs={{0,3},{1,2},{2,1},{3,0},{4,7},{5,6},{6,5},{7,4},{8,11},{9,10},{10,... | collective-permute-start | bytes 393224 | tf_op jit(solution)/shard_map/ppermute | solution.py:28
  157.8 2.6 %collective-permute-start.34 = (bf16[128,1024]{1,0:T(8,128)(2,1)S(1)}, bf16[128,1024]{1,0:T(8,128)(2,1)S(1)}, u32[]{:S(2)}, u32[]{:S(2)}) collective-permute-start(bf16[128,1024]{1,0:T(8,128)(2,1)S(1)} %get-tuple-element.27), channel_id=1, source_target_pairs={{0,3},{1,2},{2,1},{3,0},{4,7},{5,6},{6,5},{7,4},{8,11},{9,10},{10,... | collective-permute-start | bytes 786440 | tf_op jit(solution)/shard_map/ppermute | solution.py:28
  162.8 2.3 %collective-permute-start.27 = (bf16[128,512]{1,0:T(8,128)(2,1)S(1)}, bf16[128,512]{1,0:T(8,128)(2,1)S(1)}, u32[]{:S(2)}, u32[]{:S(2)}) collective-permute-start(bf16[128,512]{1,0:T(8,128)(2,1)S(1)} %get-tuple-element.24), channel_id=1, source_target_pairs={{0,2},{1,3},{2,0},{3,1},{4,6},{5,7},{6,4},{7,5},{8,10},{9,11},{10,... | collective-permute-start | bytes 393224 | tf_op jit(solution)/shard_map/ppermute | solution.py:28
  165.1 12.5 %collective-permute-done.26.refs_2_ = bf16[128,512]{1,0:T(8,128)(2,1)S(1)} collective-permute-done((bf16[128,512]{1,0:T(8,128)(2,1)S(1)}, bf16[128,512]{1,0:T(8,128)(2,1)S(1)}, u32[]{:S(2)}, u32[]{:S(2)}) %collective-permute-start.26) | collective-permute-done | bytes 131104 | tf_op jit(solution)/shard_map/ppermute | solution.py:28
  (126 shorter events, 48.2 us)
Async XLA Ops:
  11.7 38.7 %collective-permute-start.5 = (bf16[128,2048]{1,0:T(8,128)(2,1)S(1)}, bf16[128,2048]{1,0:T(8,128)(2,1)S(1)}, u32[]{:S(2)}, u32[]{:S(2)}) collective-permute-start(bf16[128,2048]{1,0:T(8,128)(2,1)S(1)} %copy-done.8), channel_id=1, source_target_pairs={{0,1},{1,0},{2,3},{3,2},{4,5},{5,4},{6,7},{7,6},{8,9},{9,8},{10,11... | collective-permute-start | bytes 1572872 | tf_op jit(solution)/shard_map/ppermute | solution.py:28
  12.1 38.3 %collective-permute-start.6 = (bf16[128,2048]{1,0:T(8,128)(2,1)S(1)}, bf16[128,2048]{1,0:T(8,128)(2,1)S(1)}, u32[]{:S(2)}, u32[]{:S(2)}) collective-permute-start(bf16[128,2048]{1,0:T(8,128)(2,1)S(1)} %copy-done.8), channel_id=1, source_target_pairs={{0,3},{1,2},{2,1},{3,0},{4,7},{5,6},{6,5},{7,4},{8,11},{9,10},{10,... | collective-permute-start | bytes 1572872 | tf_op jit(solution)/shard_map/ppermute | solution.py:28
  15.0 35.4 %collective-permute-start.7 = (bf16[128,2048]{1,0:T(8,128)(2,1)S(1)}, bf16[128,2048]{1,0:T(8,128)(2,1)S(1)}, u32[]{:S(2)}, u32[]{:S(2)}) collective-permute-start(bf16[128,2048]{1,0:T(8,128)(2,1)S(1)} %copy-done.8), channel_id=1, source_target_pairs={{0,2},{1,3},{2,0},{3,1},{4,6},{5,7},{6,4},{7,5},{8,10},{9,11},{10,... | collective-permute-start | bytes 1572872 | tf_op jit(solution)/shard_map/ppermute | solution.py:28
  15.8 17.3 %collective-permute-start.3 = (bf16[512,256]{1,0:T(8,128)(2,1)S(1)}, bf16[512,256]{1,0:T(8,128)(2,1)S(1)}, u32[]{:S(2)}, u32[]{:S(2)}) collective-permute-start(bf16[512,256]{1,0:T(8,128)(2,1)S(1)} %shard_map.118.a0), channel_id=1, source_target_pairs={{0,3},{1,2},{2,1},{3,0},{4,7},{5,6},{6,5},{7,4},{8,11},{9,10},{10,... | collective-permute-start | bytes 786440 | tf_op jit(solution)/shard_map/ppermute | solution.py:28
  17.9 32.5 %collective-permute-start.4 = (bf16[512,256]{1,0:T(8,128)(2,1)S(1)}, bf16[512,256]{1,0:T(8,128)(2,1)S(1)}, u32[]{:S(2)}, u32[]{:S(2)}) collective-permute-start(bf16[512,256]{1,0:T(8,128)(2,1)S(1)} %shard_map.118.a0), channel_id=1, source_target_pairs={{0,2},{1,3},{2,0},{3,1},{4,6},{5,7},{6,4},{7,5},{8,10},{9,11},{10,... | collective-permute-start | bytes 786440 | tf_op jit(solution)/shard_map/ppermute | solution.py:28
  33.1 24.0 %collective-permute-start.9 = (bf16[64,2176]{1,0:T(8,128)(2,1)S(1)}, bf16[64,2176]{1,0:T(8,128)(2,1)S(1)}, u32[]{:S(2)}, u32[]{:S(2)}) collective-permute-start(bf16[64,2176]{1,0:T(8,128)(2,1)S(1)} %get-tuple-element.20), channel_id=1, source_target_pairs={{0,4},{4,0},{8,12},{12,8},{16,20},{20,16},{24,28},{28,24},{32,36},... | collective-permute-start | bytes 835592 | tf_op jit(solution)/shard_map/ppermute | solution.py:28
  57.0 62.8 %collective-permute-start.8 = (bf16[512,2048]{1,0:T(8,128)(2,1)S(1)}, bf16[512,2048]{1,0:T(8,128)(2,1)S(1)}, u32[]{:S(2)}, u32[]{:S(2)}) collective-permute-start(bf16[512,2048]{1,0:T(8,128)(2,1)S(1)} %shard_map.119.mine.normed), channel_id=1, source_target_pairs={{0,4},{4,0},{8,12},{12,8},{16,20},{20,16},{24,28},{28,24},{32,36},... | collective-permute-start | bytes 6291464 | tf_op jit(solution)/shard_map/ppermute | solution.py:28
  63.0 14.4 %collective-permute-start.11 = (bf16[64,2176]{1,0:T(8,128)(2,1)S(1)}, bf16[64,2176]{1,0:T(8,128)(2,1)S(1)}, u32[]{:S(2)}, u32[]{:S(2)}) collective-permute-start(bf16[64,2176]{1,0:T(8,128)(2,1)S(1)} %get-tuple-element.34), channel_id=1, source_target_pairs={{0,24},{4,28},{8,16},{12,20},{16,8},{20,12},{24,0},{28,4},{32,56},... | collective-permute-start | bytes 835592 | tf_op jit(solution)/shard_map/ppermute | solution.py:28
  65.1 16.2 %collective-permute-start.12 = (bf16[64,2176]{1,0:T(8,128)(2,1)S(1)}, bf16[64,2176]{1,0:T(8,128)(2,1)S(1)}, u32[]{:S(2)}, u32[]{:S(2)}) collective-permute-start(bf16[64,2176]{1,0:T(8,128)(2,1)S(1)} %get-tuple-element.34), channel_id=1, source_target_pairs={{0,16},{4,20},{8,24},{12,28},{16,0},{20,4},{24,8},{28,12},{32,48},... | collective-permute-start | bytes 835592 | tf_op jit(solution)/shard_map/ppermute | solution.py:28
  66.2 17.4 %collective-permute-start.17 = (bf16[64,2176]{1,0:T(8,128)(2,1)S(1)}, bf16[64,2176]{1,0:T(8,128)(2,1)S(1)}, u32[]{:S(2)}, u32[]{:S(2)}) collective-permute-start(bf16[64,2176]{1,0:T(8,128)(2,1)S(1)} %get-tuple-element.33), channel_id=1, source_target_pairs={{0,32},{4,36},{8,40},{12,44},{16,48},{20,52},{24,56},{28,60},{32,0... | collective-permute-start | bytes 835592 | tf_op jit(solution)/shard_map/ppermute | solution.py:28
  70.5 13.3 %collective-permute-start.18 = (bf16[64,2176]{1,0:T(8,128)(2,1)S(1)}, bf16[64,2176]{1,0:T(8,128)(2,1)S(1)}, u32[]{:S(2)}, u32[]{:S(2)}) collective-permute-start(bf16[64,2176]{1,0:T(8,128)(2,1)S(1)} %get-tuple-element.33), channel_id=1, source_target_pairs={{0,96},{4,100},{8,104},{12,108},{16,112},{20,116},{24,120},{28,124... | collective-permute-start | bytes 835592 | tf_op jit(solution)/shard_map/ppermute | solution.py:28
  81.4 21.1 %collective-permute-start.13 = (bf16[256,1408]{1,0:T(8,128)(2,1)S(1)}, bf16[256,1408]{1,0:T(8,128)(2,1)S(1)}, u32[]{:S(2)}, u32[]{:S(2)}) collective-permute-start(bf16[256,1408]{1,0:T(8,128)(2,1)S(1)} %pad_maximum_fusion.refs_0_), channel_id=1, source_target_pairs={{0,32},{4,36},{8,40},{12,44},{16,48},{20,52},{24,56},{28,60},{32,0... | collective-permute-start | bytes 2162696 | tf_op jit(solution)/shard_map/ppermute | solution.py:28
  83.6 20.0 %collective-permute-start.14 = (bf16[256,1408]{1,0:T(8,128)(2,1)S(1)}, bf16[256,1408]{1,0:T(8,128)(2,1)S(1)}, u32[]{:S(2)}, u32[]{:S(2)}) collective-permute-start(bf16[256,1408]{1,0:T(8,128)(2,1)S(1)} %pad_maximum_fusion.refs_0_), channel_id=1, source_target_pairs={{0,96},{4,100},{8,104},{12,108},{16,112},{20,116},{24,120},{28,124... | collective-permute-start | bytes 2162696 | tf_op jit(solution)/shard_map/ppermute | solution.py:28
  88.8 16.1 %collective-permute-start.20 = (bf16[256,1408]{1,0:T(8,128)(2,1)S(1)}, bf16[256,1408]{1,0:T(8,128)(2,1)S(1)}, u32[]{:S(2)}, u32[]{:S(2)}) collective-permute-start(bf16[256,1408]{1,0:T(8,128)(2,1)S(1)} %pad_maximum_fusion.1.refs_5_), channel_id=1, source_target_pairs={{0,8},{4,12},{8,0},{12,4},{16,24},{20,28},{24,16},{28,20},{32,40},... | collective-permute-start | bytes 2162696 | tf_op jit(solution)/shard_map/ppermute | solution.py:28
  90.7 18.1 %collective-permute-start.21 = (bf16[256,1408]{1,0:T(8,128)(2,1)S(1)}, bf16[256,1408]{1,0:T(8,128)(2,1)S(1)}, u32[]{:S(2)}, u32[]{:S(2)}) collective-permute-start(bf16[256,1408]{1,0:T(8,128)(2,1)S(1)} %pad_maximum_fusion.1.refs_5_), channel_id=1, source_target_pairs={{0,24},{4,28},{8,16},{12,20},{16,8},{20,12},{24,0},{28,4},{32,56},... | collective-permute-start | bytes 2162696 | tf_op jit(solution)/shard_map/ppermute | solution.py:28
  112.3 24.1 %collective-permute-start.36 = (bf16[256,768]{1,0:T(8,128)(2,1)S(1)}, bf16[256,768]{1,0:T(8,128)(2,1)S(1)}, u32[]{:S(2)}, u32[]{:S(2)}) collective-permute-start(bf16[256,768]{1,0:T(8,128)(2,1)S(1)} %pad_maximum_fusion.2.refs_0_), channel_id=1, source_target_pairs={{0,64},{4,68},{8,72},{12,76},{16,80},{20,84},{24,88},{28,92},{32,9... | collective-permute-start | bytes 1179656 | tf_op jit(solution)/shard_map/ppermute | solution.py:28
  113.9 16.2 %collective-permute-start.28 = (bf16[256,768]{1,0:T(8,128)(2,1)S(1)}, bf16[256,768]{1,0:T(8,128)(2,1)S(1)}, u32[]{:S(2)}, u32[]{:S(2)}) collective-permute-start(bf16[256,768]{1,0:T(8,128)(2,1)S(1)} %pad_maximum_fusion.2.refs_0_), channel_id=1, source_target_pairs={{0,32},{4,36},{8,40},{12,44},{16,48},{20,52},{24,56},{28,60},{32,0... | collective-permute-start | bytes 1179656 | tf_op jit(solution)/shard_map/ppermute | solution.py:28
  116.4 15.3 %collective-permute-start.29 = (bf16[256,768]{1,0:T(8,128)(2,1)S(1)}, bf16[256,768]{1,0:T(8,128)(2,1)S(1)}, u32[]{:S(2)}, u32[]{:S(2)}) collective-permute-start(bf16[256,768]{1,0:T(8,128)(2,1)S(1)} %pad_maximum_fusion.2.refs_0_), channel_id=1, source_target_pairs={{0,96},{4,100},{8,104},{12,108},{16,112},{20,116},{24,120},{28,124... | collective-permute-start | bytes 1179656 | tf_op jit(solution)/shard_map/ppermute | solution.py:28
  132.7 22.0 %collective-permute-start.32 = (bf16[512,1024]{1,0:T(8,128)(2,1)S(1)}, bf16[512,1024]{1,0:T(8,128)(2,1)S(1)}, u32[]{:S(2)}, u32[]{:S(2)}) collective-permute-start(bf16[512,1024]{1,0:T(8,128)(2,1)S(1)} %shard_map.124), channel_id=1, source_target_pairs={{0,4},{4,0},{8,12},{12,8},{16,20},{20,16},{24,28},{28,24},{32,36},... | collective-permute-start | bytes 3145736 | tf_op jit(solution)/shard_map/ppermute | solution.py:28
  155.8 21.7 %collective-permute-start.33 = (bf16[128,1024]{1,0:T(8,128)(2,1)S(1)}, bf16[128,1024]{1,0:T(8,128)(2,1)S(1)}, u32[]{:S(2)}, u32[]{:S(2)}) collective-permute-start(bf16[128,1024]{1,0:T(8,128)(2,1)S(1)} %get-tuple-element.26), channel_id=1, source_target_pairs={{0,1},{1,0},{2,3},{3,2},{4,5},{5,4},{6,7},{7,6},{8,9},{9,8},{10,11... | collective-permute-start | bytes 786440 | tf_op jit(solution)/shard_map/ppermute | solution.py:28
  157.8 19.8 %collective-permute-start.34 = (bf16[128,1024]{1,0:T(8,128)(2,1)S(1)}, bf16[128,1024]{1,0:T(8,128)(2,1)S(1)}, u32[]{:S(2)}, u32[]{:S(2)}) collective-permute-start(bf16[128,1024]{1,0:T(8,128)(2,1)S(1)} %get-tuple-element.27), channel_id=1, source_target_pairs={{0,3},{1,2},{2,1},{3,0},{4,7},{5,6},{6,5},{7,4},{8,11},{9,10},{10,... | collective-permute-start | bytes 786440 | tf_op jit(solution)/shard_map/ppermute | solution.py:28
  160.4 17.1 %collective-permute-start.35 = (bf16[128,1024]{1,0:T(8,128)(2,1)S(1)}, bf16[128,1024]{1,0:T(8,128)(2,1)S(1)}, u32[]{:S(2)}, u32[]{:S(2)}) collective-permute-start(bf16[128,1024]{1,0:T(8,128)(2,1)S(1)} %get-tuple-element.28), channel_id=1, source_target_pairs={{0,2},{1,3},{2,0},{3,1},{4,6},{5,7},{6,4},{7,5},{8,10},{9,11},{10,... | collective-permute-start | bytes 786440 | tf_op jit(solution)/shard_map/ppermute | solution.py:28
  161.8 15.7 %collective-permute-start.26 = (bf16[128,512]{1,0:T(8,128)(2,1)S(1)}, bf16[128,512]{1,0:T(8,128)(2,1)S(1)}, u32[]{:S(2)}, u32[]{:S(2)}) collective-permute-start(bf16[128,512]{1,0:T(8,128)(2,1)S(1)} %get-tuple-element.23), channel_id=1, source_target_pairs={{0,3},{1,2},{2,1},{3,0},{4,7},{5,6},{6,5},{7,4},{8,11},{9,10},{10,... | collective-permute-start | bytes 393224 | tf_op jit(solution)/shard_map/ppermute | solution.py:28
  162.8 14.7 %collective-permute-start.27 = (bf16[128,512]{1,0:T(8,128)(2,1)S(1)}, bf16[128,512]{1,0:T(8,128)(2,1)S(1)}, u32[]{:S(2)}, u32[]{:S(2)}) collective-permute-start(bf16[128,512]{1,0:T(8,128)(2,1)S(1)} %get-tuple-element.24), channel_id=1, source_target_pairs={{0,2},{1,3},{2,0},{3,1},{4,6},{5,7},{6,4},{7,5},{8,10},{9,11},{10,... | collective-permute-start | bytes 393224 | tf_op jit(solution)/shard_map/ppermute | solution.py:28
  (30 other events, 315.9 us)

commit v2 on v1

v2 whole, which is shorter than its diff:
```python
import jax
import jax.numpy as jnp
from jax import lax
from jax.experimental import pallas as pl
from jax.experimental.pallas import tpu as pltpu
from jax.sharding import PartitionSpec as P


HEAD = 128
HALF = 128
ALPHA = 2.0**0.5
EPS = 1e-05
NEGATIVE = -1e30
BF, F32 = jnp.bfloat16, jnp.float32

ROWS = 512
OWN = 128
D = 2048
FFH = 704
GU = 2 * FFH
DN = 768
ORDER = (0, 1, 3, 2)
SP_Y, SP_Z = 2, 8


def swap(value, axis, mask):
    count = lax.axis_size(axis)
    return lax.ppermute(value, axis, [(i, i ^ mask) for i in range(count)])


def ring(value, axis, low):
    return [value] + [swap(value, axis, low * m) for m in ORDER[1:]]


def call(body, outs, flops, bytes_accessed, args, scratch=(), space=pltpu.VMEM, vmem_mib=20):
    vmem = pl.BlockSpec(memory_space=pltpu.VMEM)
    return pl.pallas_call(
        body,
        out_shape=outs,
        in_specs=[pl.BlockSpec(memory_space=space)] * len(args),
        out_specs=jax.tree.map(lambda _: vmem, outs),
        scratch_shapes=list(scratch),
        compiler_params=pltpu.CompilerParams(vmem_limit_bytes=vmem_mib << 20),
        cost_estimate=pl.CostEstimate(
            flops=flops, bytes_accessed=bytes_accessed, transcendentals=0
        ),
    )(*args)


def shape(dims, dtype=BF):
    return jax.ShapeDtypeStruct(dims, dtype)


def pack_body(
    gate, up, down, q, k, v, docs, sinks, *refs
):
    keep, send, side, far, q_o, k_o, v_o, docs_o, sinks_o, gate_v, up_v, down_v, sems = refs
    moves = [(gate, gate_v), (up, up_v), (down, down_v), (k, k_o), (v, v_o), (docs, docs_o)]
    moves += [(q, q_o), (sinks, sinks_o)]
    copies = [pltpu.make_async_copy(*m, sems.at[i]) for i, m in enumerate(moves)]
    for copy in copies:
        copy.start()
    zero = lax.axis_index("sp") % 2 == 0
    low = lax.broadcasted_iota(jnp.int32, (64, GU), 1) < FFH
    for copy in copies[:2]:
        copy.wait()
    g, u = gate_v[...].astype(F32), up_v[...].astype(F32)
    first = jnp.where(low, g, pltpu.roll(u, FFH, 1))
    second = jnp.where(low, pltpu.roll(g, FFH, 1), u)
    keep[:, :GU] = jnp.where(zero, first, second).astype(BF)
    send[:, :GU] = jnp.where(zero, second, first).astype(BF)
    copies[2].wait()
    d = down_v[...].astype(F32)
    d0 = jnp.where(low, d, 0.0)[:, :DN]
    d1 = jnp.where(low, pltpu.roll(d, FFH, 1), 0.0)[:, :DN]
    keep[:, GU:] = jnp.where(zero, d0, d1).astype(BF)
    send[:, GU:] = jnp.where(zero, d1, d0).astype(BF)
    for copy in copies[3:]:
        copy.wait()
    a, b = slice(0, HALF), slice(ROWS - HALF, ROWS)
    for out, end in ((side, zero), (far, jnp.logical_not(zero))):
        out[:HALF, :HEAD] = jnp.where(end, k_o[b, :], k_o[a, :])
        out[:HALF, HEAD:] = jnp.where(end, v_o[b, :], v_o[a, :])
        d = docs_o[...].astype(F32)
        d = jnp.where(end, d[:, b], d[:, a]).astype(BF)
        d = jnp.broadcast_to(d, (8, HALF))
        out[HALF:, :HEAD] = d
        out[HALF:, HEAD:] = d


def attend_body(q, k, v, docs, sinks, side, far, o0, o1, o3, o2, kv, drow):
    sp = lax.axis_index("sp")
    core = sp % 2
    zero = core == 0
    before = jnp.where(zero, far[...].astype(F32), side[...].astype(F32))
    after = jnp.where(zero, side[...].astype(F32), far[...].astype(F32))
    kv[0:HALF, :] = before[:HALF].astype(BF)
    kv[HALF : HALF + ROWS, :HEAD] = k[...]
    kv[HALF : HALF + ROWS, HEAD:] = v[...]
    kv[HALF + ROWS :, :] = after[:HALF].astype(BF)
    drow[:, 0:HALF] = jnp.where(sp == 0, -1.0, before[HALF:, :HALF])
    drow[:, HALF : HALF + ROWS] = jnp.broadcast_to(docs[...].astype(F32), (8, ROWS))
    drow[:, HALF + ROWS :] = jnp.where(
        sp == lax.axis_size("sp") - 1, -1.0, after[HALF:, :HALF]
    )
    span = 3 * HALF
    row = lax.broadcasted_iota(jnp.int32, (HALF, span), 0)
    col = lax.broadcasted_iota(jnp.int32, (HALF, span), 1)
    near = jnp.abs(col - HALF - row) <= HALF
    for mask, out in zip(ORDER, (o0, o1, o3, o2)):
        start = pl.multiple_of((lax.axis_index("tp") ^ mask) * HALF, HALF)
        own = pl.ds(pl.multiple_of(start + HALF, HALF), HALF)
        window = pl.ds(start, span)
        dq = jnp.broadcast_to(drow[0:1, own], (HALF, HALF)).T
        same = jnp.concatenate([dq, dq, dq], 1) == drow[0:1, window]
        ok = near & same
        keys = kv[window, :HEAD]
        vals = kv[window, HEAD:]
        for h in range(2):
            cols = slice(h * HEAD, (h + 1) * HEAD)
            s = lax.dot_general(
                q[pl.ds(start, HALF), cols],
                keys,
                (((1,), (1,)), ((), ())),
                preferred_element_type=F32,
            ) * HEAD ** (-0.5)
            s = jnp.where(ok, s, NEGATIVE)
            sink = sinks[0:1, h : h + 1]
            top = jnp.maximum(jnp.max(s, -1, keepdims=True), sink)
            w = jnp.exp(s - top)
            total = jnp.sum(w, -1, keepdims=True) + jnp.exp(sink - top)
            o = jnp.dot(w.astype(BF), vals, preferred_element_type=F32)
            out[:, cols] = (o / total).astype(BF)


def normalised(value):
    average = jnp.mean(value, -1, keepdims=True)
    centred = value - average
    variance = jnp.mean(centred * centred, -1, keepdims=True)
    return centred * lax.rsqrt(variance + EPS)


def chip(rz, ry):
    sp = lax.axis_index("sp")
    y, z = (sp // SP_Y) % 4, sp // SP_Z
    return pl.multiple_of(((z ^ rz) * 4 + (y ^ ry)) * 128, 128)


def norm_body(a0, a1, a3, a2, w_out, res, gain, out, nat, rot):
    x = lax.axis_index("tp")
    for n in range(0, D, 256):
        acc = ALPHA * res[:, n : n + 256].astype(F32)
        for mask, a in zip(ORDER, (a0, a1, a3, a2)):
            w = w_out[pl.ds(pl.multiple_of((x ^ mask) * 256, 256), 256), n : n + 256]
            acc = acc + jnp.dot(a[...], w, preferred_element_type=F32)
        nat[:, n : n + 256] = acc
    for s in range(0, OWN, 32):
        nat[s : s + 32, :] = normalised(nat[s : s + 32, :]) * gain[...]
    for t in range(0, D, 128):
        rot[:, t : t + 128] = pltpu.roll(nat[:, t : t + 128], 64, 1)
    low = lax.broadcasted_iota(jnp.int32, (OWN, 128), 1) < 64
    for i in range(4):
        for j in (0, 2):
            a, b = (pl.ds(chip(ORDER[i], ORDER[k]), 128) for k in (j, j + 1))
            dst = (i * 4 + j) * 64
            out[:, dst : dst + 128] = jnp.where(low, nat[:, a], rot[:, b]).astype(BF)
            a, b = (pl.ds(chip(ORDER[k], ORDER[i]), 128) for k in (j, j + 1))
            dst += 1024
            out[:, dst : dst + 128] = jnp.where(low, rot[:, a], nat[:, b]).astype(BF)


def product(rows, pieces, spans, acc, store):
    lhs = jnp.concatenate(
        [jnp.concatenate([r[:, a:b] for r in rows], 0) for a, b in spans], 1
    )
    for n in range(0, GU, 256):
        m = min(n + 256, GU)
        w = jnp.concatenate([p[:, n:m] for p in pieces], 0)
        t = jnp.dot(lhs, w, preferred_element_type=F32)
        store[:, n:m] = t if acc is None else acc[:, n:m] + t


def early_body(*refs):
    product(refs[:5], refs[5:17], ((0, 768), (1024, 1792)), None, refs[17])


def hidden_body(*refs):
    rows, pieces, early, out, acc = refs[:5], refs[5:9], refs[9], refs[10], refs[11]
    product(rows, pieces, ((768, 1024), (1792, 2048)), early, acc)
    live = lax.broadcasted_iota(jnp.int32, (64, DN), 1) < FFH
    for s in range(0, ROWS, 64):
        v = acc[s : s + 64, :]
        up = pltpu.roll(v, FFH, 1)[:, :DN]
        gate = v[:, :DN]
        h = gate / (1.0 + jnp.exp(-gate)) * up
        out[s : s + 64, :] = jnp.where(live, h, 0.0).astype(BF)


def down_parts(h, pieces):
    for i in range(0, len(pieces), 2):
        p = jnp.concatenate([r[:, GU:] for r in pieces[i : i + 2]], 0)
        at = i * 128
        yield (
            at,
            at + 256,
            lax.dot_general(h[...], p, (((1,), (1,)), ((), ())), preferred_element_type=F32),
        )


def give_body(h, *refs):
    pieces, out = refs[:-1], refs[-1]
    for a, b, v in down_parts(h, pieces):
        out[:, a:b] = v.astype(BF)


def take_body(h, theirs, *refs):
    pieces, (own, left, right, left_keep, right_keep) = refs[:-5], refs[-5:]
    half = own.shape[1] // 2
    for at, end, v in down_parts(h, pieces):
        v = v + theirs[:, at:end].astype(F32)
        b0, b1, b3, b2 = (v[k * OWN : (k + 1) * OWN, :] for k in range(4))
        own[:, at:end] = b0
        send, keep, near, away = (
            (left, left_keep, b1, b3) if at < half else (right, right_keep, b3, b1)
        )
        cols = slice(at % half, at % half + end - at)
        send[:OWN, cols] = near.astype(BF)
        send[OWN:, cols] = b2.astype(BF)
        keep[:, cols] = away


def fold_body(own, left, right, left_keep, right_keep, total, left_out, right_out):
    half = own.shape[1] // 2
    total[:, :half] = own[:, :half] + left[:OWN, :].astype(F32)
    total[:, half:] = own[:, half:] + right[:OWN, :].astype(F32)
    left_out[...] = (left_keep[...] + left[OWN:, :].astype(F32)).astype(BF)
    right_out[...] = (right_keep[...] + right[OWN:, :].astype(F32)).astype(BF)


def final_body(normed, gain, *refs):
    parts, out, pre = refs[:6], refs[6], refs[7]
    for c, (first, width) in enumerate(((0, 512), (512, 512))):
        total, *last = parts[3 * c : 3 * c + 3]
        for kind in range(2):
            dst = slice(kind * 1024 + first, kind * 1024 + first + width)
            n = normed[:, dst].astype(F32)
            v = total[:, kind * width : (kind + 1) * width] + last[kind][...].astype(F32)
            pre[:, dst] = ALPHA * n + v
    pre[...] = normalised(pre[...])
    low = lax.broadcasted_iota(jnp.int32, (OWN, 128), 1) < 64
    for i in range(4):
        for j in range(4):
            p, q = 4 * i + j, 4 * j + i
            a = pre[:, (p // 2) * 128 : (p // 2) * 128 + 128]
            b = pre[:, 1024 + (q // 2) * 128 : 1024 + (q // 2) * 128 + 128]
            if p % 2 == 1:
                a = pltpu.roll(a, 64, 1)
            if q % 2 == 0:
                b = pltpu.roll(b, 64, 1)
            at = pl.ds(chip(ORDER[i], ORDER[j]), 128)
            out[:, at] = (jnp.where(low, a, b) * gain[:, at]).astype(BF)


def spread(low_half, high_half, axis, low):
    one = swap(low_half, axis, low), swap(high_half, axis, low)
    three = swap(low_half, axis, 3 * low), swap(high_half, axis, 3 * low)
    two = swap(one[0], axis, 3 * low), swap(three[1], axis, low)
    return (low_half, high_half, *one, *three, *two)


def per_device(
    queries,
    keys,
    values,
    doc_ids,
    sink_logit,
    residual_in,
    w_out,
    gain_one,
    w_gate,
    w_up,
    w_down,
    gain_two,
):
    core = lax.axis_index("sp") % 2
    local = (queries, keys, values, doc_ids.reshape(1, ROWS), sink_logit.reshape(1, 2))
    keep, send, inner, outer, *local = call(
        pack_body,
        (shape((64, GU + DN)),) * 2
        + (shape((HALF + 8, 2 * HEAD)),) * 2
        + tuple(shape(a.shape, a.dtype) for a in local),
        10**6,
        10**6,
        tuple(
            pltpu.with_memory_space_constraint(a, pltpu.HBM)
            for a in (w_gate, w_up, w_down.T, *local)
        ),
        [pltpu.VMEM((64, GU), BF)] * 3 + [pltpu.SemaphoreType.DMA((8,))],
        pltpu.HBM,
    )
    recv = swap(send, "sp", 1)
    from_0 = jnp.where(core == 0, keep, recv)
    from_1 = jnp.where(core == 0, recv, keep)

    side = swap(inner, "sp", 1)
    count = lax.axis_size("sp")
    pairs = [(i, i + 1) for i in range(1, count - 1, 2)]
    far = lax.ppermute(outer, "sp", pairs + [(b, a) for a, b in pairs])

    def columns(origin, near, across):
        units = ring(origin, "sp", near)
        halves = (jnp.concatenate(units[i : i + 2], 0) for i in (0, 2))
        return spread(*halves, "sp", across)

    all_a = columns(from_0, SP_Y, SP_Z)
    all_b = columns(from_1, SP_Z, SP_Y)

    attended = call(
        attend_body,
        (shape((OWN, 256)),) * 4,
        4 * ROWS * 256 * 384 * 8,
        10**6,
        (*local, side, far),
        (pltpu.VMEM((ROWS + 2 * HALF, 256), BF), pltpu.VMEM((8, ROWS + 2 * HALF), F32)),
    )
    atts = [swap(a, "tp", m) if m else a for m, a in zip(ORDER, attended)]
    normed = call(
        norm_body,
        shape((OWN, D)),
        2 * OWN * 1024 * D * 4,
        10**7,
        (*atts, w_out, residual_in, gain_one.reshape(1, D)),
        (pltpu.VMEM((OWN, D), F32),) * 2,
    )
    x1, x3 = swap(normed, "tp", 1), swap(normed, "tp", 3)
    mid = OWN // 2
    rows = (normed, x1, x3, swap(x1[:mid], "tp", 3), swap(x3[mid:], "tp", 1))
    others = [swap(r, "sp", 1) for r in rows]

    def hidden_of(r):
        early = call(
            early_body,
            shape((ROWS, GU), F32),
            2 * ROWS * 1536 * GU,
            10**7,
            (*r, *all_a[:6], *all_b[:6]),
        )
        return call(
            hidden_body,
            shape((ROWS, DN)),
            2 * ROWS * 512 * GU,
            10**7,
            (*r, *all_a[6:], *all_b[6:], early),
            (pltpu.VMEM((ROWS, GU), F32),),
        )

    own_hidden, other_hidden = hidden_of(rows), hidden_of(others)
    sums = []
    chunks = [slice(0, 4), slice(4, 8)]
    for part_of in chunks:
        pieces = (*all_a[part_of], *all_b[part_of])
        width = sum(p.shape[0] for p in pieces)
        flops = 2 * ROWS * DN * width
        part = call(give_body, shape((ROWS, width)), flops, 10**6, (other_hidden, *pieces))
        theirs = swap(part, "sp", 1)
        half = width // 2
        own, left, right, *keeps = call(
            take_body,
            (shape((OWN, width), F32),)
            + (shape((2 * OWN, half)),) * 2
            + (shape((OWN, half), F32),) * 2,
            flops,
            10**6,
            (own_hidden, theirs, *pieces),
        )
        left, right = swap(left, "tp", 1), swap(right, "tp", 3)
        own, left, right = call(
            fold_body,
            (shape((OWN, width), F32),) + (shape((OWN, half)),) * 2,
            10**6,
            10**6,
            (own, left, right, *keeps),
        )
        sums += [own, swap(left, "tp", 3), swap(right, "tp", 1)]
    return call(
        final_body,
        shape((OWN, D)),
        10**6,
        10**6,
        (normed, gain_two.reshape(1, D), *sums),
        (pltpu.VMEM((OWN, D), F32),),
    )


def solution(mesh):
    in_specs = (
        P("sp", "tp"),
        P("sp", "tp"),
        P("sp", "tp"),
        P("sp"),
        P("tp"),
        P(("sp", "tp"), None),
        P(),
        P(),
        P("sp", "tp"),
        P("sp", "tp"),
        P("tp", "sp"),
        P(),
    )
    out_specs = P(("sp", "tp"), None)
    return jax.shard_map(
        per_device, mesh=mesh, in_specs=in_specs, out_specs=out_specs, check_vma=False
    )
```

time: 180 us -> 135 us (0.75)
  starting transfers between devices: 86 us -> 51.6 us
  local copies, waits for them, and re-layouts: 5.26 us -> 0.15 us
  Pallas kernels: 22.9 us -> 19.3 us
    ppermute x41 -> x42, starting transfers between devices: 85.3 us -> 50.9 us  [swap(): return lax.ppermute(value, axis, [(i, i ^ mask) for i in range(count)])]
    unnamed x24 -> x10, local copies, waits for them, and re-layouts: 4.13 us -> 0.06 us
    pallas_call x11 -> x14, Pallas kernels: 22.9 us -> 19.3 us  [call(): pl.pallas_call(body, out_shape=outs, in_specs=[pl.BlockSpec(memory_space=...]
    ppermute x41 -> x42, waiting for transfers between devices: 63.7 us -> 63 us  [swap(): return lax.ppermute(value, axis, [(i, i ^ mask) for i in range(count)])]
  transfers between devices with their start and end apart: 42 -> 43, of which waited for: 13 -> 22; matrix products, arithmetic and copies ran while one was open for 0% -> 0% of each run, Pallas kernels for 10% -> 11%
where the time goes in v2:
time: 135 us; the launch traced here: 134 us
  waiting for transfers between devices  63 us (47%)
  starting transfers between devices  51.6 us (38%)
  Pallas kernels  19.3 us (14%)
    ppermute x42, waiting for transfers between devices, swap(): return lax.ppermute(value, axis, [(i, i ^ mask) for i in range(count)])  63 us
    ppermute x42, starting transfers between devices, swap(): return lax.ppermute(value, axis, [(i, i ^ mask) for i in range(count)])  50.9 us
    pallas_call x14, Pallas kernels, call(): pl.pallas_call(body, out_shape=outs, in_specs=[pl.BlockSpec(memory_space=...  19.3 us
  transfers between devices with their start and end apart: 43, of which 22 were waited for; matrix products, arithmetic and copies ran while one was open for 0% of the time, Pallas kernels for 11%

profile of v2, /device:TPU:0, one launch (start us, length us, event | category | flops | bytes accessed | tf_op | source)
XLA Modules:
  0.0 134.4 jit_solution(6438500668042215893)
XLA Ops:
  3.1 2.7 %collective-permute-start.10 = (bf16[64,2176]{1,0:T(8,128)(2,1)S(1)}, bf16[64,2176]{1,0:T(8,128)(2,1)S(1)}, u32[]{:S(2)}, u32[]{:S(2)}) collective-permute-start(bf16[64,2176]{1,0:T(8,128)(2,1)S(1)} %get-tuple-element.64), channel_id=1, source_target_pairs={{0,8},{4,12},{8,0},{12,4},{16,24},{20,28},{24,16},{28,20},{32,40},... | collective-permute-start | bytes 835592 | tf_op jit(solution)/shard_map/ppermute | solution.py:28
  5.8 3.0 %shard_map.119 = (bf16[128,256]{1,0:T(8,128)(2,1)S(1)}, bf16[128,256]{1,0:T(8,128)(2,1)S(1)}, bf16[128,256]{1,0:T(8,128)(2,1)S(1)}, bf16[128,256]{1,0:T(8,128)(2,1)S(1)}) custom-call(bf16[512,256]{1,0:T(8,128)(2,1)S(1)} %get-tuple-element.34.q, bf16[512,128]{1,0:T(8,128)(2,1)S(1)} %get-tuple-element.35.k, bf16[512,128]{1,0:T(8,128)(2,1)S(1)} %get-tuple-element.36.v, ...), custom_call_target="tpu_custom_call" | custom-call | flops 1610612736 | bytes 1000000 | tf_op jit(solution)/shard_map/pallas_call | solution.py:37
  13.2 2.8 %collective-permute-done.3.a3 = bf16[128,256]{1,0:T(8,128)(2,1)S(1)} collective-permute-done((bf16[128,256]{1,0:T(8,128)(2,1)S(1)}, bf16[128,256]{1,0:T(8,128)(2,1)S(1)}, u32[]{:S(2)}, u32[]{:S(2)}) %collective-permute-start.3) | collective-permute-done | bytes 65568 | tf_op jit(solution)/shard_map/ppermute | solution.py:28
  16.0 2.7 %collective-permute-done.4.a2 = bf16[128,256]{1,0:T(8,128)(2,1)S(1)} collective-permute-done((bf16[128,256]{1,0:T(8,128)(2,1)S(1)}, bf16[128,256]{1,0:T(8,128)(2,1)S(1)}, u32[]{:S(2)}, u32[]{:S(2)}) %collective-permute-start.4) | collective-permute-done | bytes 65568 | tf_op jit(solution)/shard_map/ppermute | solution.py:28
  21.6 4.9 %collective-permute-start.13 = (bf16[64,2176]{1,0:T(8,128)(2,1)S(1)}, bf16[64,2176]{1,0:T(8,128)(2,1)S(1)}, u32[]{:S(2)}, u32[]{:S(2)}) collective-permute-start(bf16[64,2176]{1,0:T(8,128)(2,1)S(1)} %get-tuple-element.64), channel_id=1, source_target_pairs={{0,24},{4,28},{8,16},{12,20},{16,8},{20,12},{24,0},{28,4},{32,56},... | collective-permute-start | bytes 835592 | tf_op jit(solution)/shard_map/ppermute | solution.py:28
  28.5 6.7 %collective-permute-done.17 = bf16[64,2176]{1,0:T(8,128)(2,1)S(1)} collective-permute-done((bf16[64,2176]{1,0:T(8,128)(2,1)S(1)}, bf16[64,2176]{1,0:T(8,128)(2,1)S(1)}, u32[]{:S(2)}, u32[]{:S(2)}) %collective-permute-start.17) | collective-permute-done | bytes 278560 | tf_op jit(solution)/shard_map/ppermute | solution.py:28
  35.7 3.9 %collective-permute-start.20 = (bf16[64,2176]{1,0:T(8,128)(2,1)S(1)}, bf16[64,2176]{1,0:T(8,128)(2,1)S(1)}, u32[]{:S(2)}, u32[]{:S(2)}) collective-permute-start(bf16[64,2176]{1,0:T(8,128)(2,1)S(1)} %get-tuple-element.63), channel_id=1, source_target_pairs={{0,96},{4,100},{8,104},{12,108},{16,112},{20,116},{24,120},{28,124... | collective-permute-start | bytes 835592 | tf_op jit(solution)/shard_map/ppermute | solution.py:28
  39.6 6.3 %collective-permute-done.20 = bf16[64,2176]{1,0:T(8,128)(2,1)S(1)} collective-permute-done((bf16[64,2176]{1,0:T(8,128)(2,1)S(1)}, bf16[64,2176]{1,0:T(8,128)(2,1)S(1)}, u32[]{:S(2)}, u32[]{:S(2)}) %collective-permute-start.20) | collective-permute-done | bytes 278560 | tf_op jit(solution)/shard_map/ppermute | solution.py:28
  47.5 2.3 %collective-permute-start.11 = (bf16[128,2176]{1,0:T(8,128)(2,1)S(1)}, bf16[128,2176]{1,0:T(8,128)(2,1)S(1)}, u32[]{:S(2)}, u32[]{:S(2)}) collective-permute-start(bf16[128,2176]{1,0:T(8,128)(2,1)S(1)} %pad_maximum_fusion.refs_5_.refs_0_), channel_id=1, source_target_pairs={{0,32},{4,36},{8,40},{12,44},{16,48},{20,52},{24,56},{28,60},{32,0... | collective-permute-start | bytes 1671176 | tf_op jit(solution)/shard_map/ppermute | solution.py:28
  50.3 2.3 %collective-permute-start.18 = (bf16[128,2176]{1,0:T(8,128)(2,1)S(1)}, bf16[128,2176]{1,0:T(8,128)(2,1)S(1)}, u32[]{:S(2)}, u32[]{:S(2)}) collective-permute-start(bf16[128,2176]{1,0:T(8,128)(2,1)S(1)} %pad_maximum_fusion.1.refs_11_.refs_4_), channel_id=1, source_target_pairs={{0,8},{4,12},{8,0},{12,4},{16,24},{20,28},{24,16},{28,20},{32,40},... | collective-permute-start | bytes 1671176 | tf_op jit(solution)/shard_map/ppermute | solution.py:28
  52.6 4.4 %collective-permute-done.21 = bf16[64,2176]{1,0:T(8,128)(2,1)S(1)} collective-permute-done((bf16[64,2176]{1,0:T(8,128)(2,1)S(1)}, bf16[64,2176]{1,0:T(8,128)(2,1)S(1)}, u32[]{:S(2)}, u32[]{:S(2)}) %collective-permute-start.21) | collective-permute-done | bytes 278560 | tf_op jit(solution)/shard_map/ppermute | solution.py:28
  57.0 2.6 %collective-permute-start.7 = (bf16[64,2048]{1,0:T(8,128)(2,1)S(1)}, bf16[64,2048]{1,0:T(8,128)(2,1)S(1)}, u32[]{:S(2)}, u32[]{:S(2)}) collective-permute-start(bf16[64,2048]{1,0:T(8,128)(2,1)S(1)} %slice.8), channel_id=1, source_target_pairs={{0,3},{1,2},{2,1},{3,0},{4,7},{5,6},{6,5},{7,4},{8,11},{9,10},{10,... | collective-permute-start | bytes 786440 | tf_op jit(solution)/shard_map/ppermute | solution.py:28
  59.8 4.7 %collective-permute-done.7.refs_3_ = bf16[64,2048]{1,0:T(8,128)(2,1)S(1)} collective-permute-done((bf16[64,2048]{1,0:T(8,128)(2,1)S(1)}, bf16[64,2048]{1,0:T(8,128)(2,1)S(1)}, u32[]{:S(2)}, u32[]{:S(2)}) %collective-permute-start.7) | collective-permute-done | bytes 262176 | tf_op jit(solution)/shard_map/ppermute | solution.py:28
  66.7 2.6 %collective-permute-done.11.refs_7_.refs_2_ = bf16[128,2176]{1,0:T(8,128)(2,1)S(1)} collective-permute-done((bf16[128,2176]{1,0:T(8,128)(2,1)S(1)}, bf16[128,2176]{1,0:T(8,128)(2,1)S(1)}, u32[]{:S(2)}, u32[]{:S(2)}) %collective-permute-start.11) | collective-permute-done | bytes 557088 | tf_op jit(solution)/shard_map/ppermute | solution.py:28
  72.4 7.4 %collective-permute-done.22.refs_16_.refs_5_ = bf16[128,2176]{1,0:T(8,128)(2,1)S(1)} collective-permute-done((bf16[128,2176]{1,0:T(8,128)(2,1)S(1)}, bf16[128,2176]{1,0:T(8,128)(2,1)S(1)}, u32[]{:S(2)}, u32[]{:S(2)}) %collective-permute-start.22) | collective-permute-done | bytes 557088 | tf_op jit(solution)/shard_map/ppermute | solution.py:28
  80.5 3.5 %collective-permute-start.12 = (bf16[128,2176]{1,0:T(8,128)(2,1)S(1)}, bf16[128,2176]{1,0:T(8,128)(2,1)S(1)}, u32[]{:S(2)}, u32[]{:S(2)}) collective-permute-start(bf16[128,2176]{1,0:T(8,128)(2,1)S(1)} %collective-permute-done.11.refs_7_.refs_2_), channel_id=1, source_target_pairs={{0,96},{4,100},{8,104},{12,108},{16,112},{20,116},{24,120},{28,124... | collective-permute-start | bytes 1671176 | tf_op jit(solution)/shard_map/ppermute | solution.py:28
  84.0 3.3 %collective-permute-done.27.refs_15_.refs_4_ = bf16[128,2176]{1,0:T(8,128)(2,1)S(1)} collective-permute-done((bf16[128,2176]{1,0:T(8,128)(2,1)S(1)}, bf16[128,2176]{1,0:T(8,128)(2,1)S(1)}, u32[]{:S(2)}, u32[]{:S(2)}) %collective-permute-start.27) | collective-permute-done | bytes 557088 | tf_op jit(solution)/shard_map/ppermute | solution.py:28
  91.0 2.6 %shard_map.123.refs_9_ = f32[512,1408]{1,0:T(8,128)S(1)} custom-call(bf16[128,2048]{1,0:T(8,128)(2,1)S(1)} %collective-permute-done.28.refs_0_, bf16[128,2048]{1,0:T(8,128)(2,1)S(1)} %collective-permute-done.29.refs_1_, bf16[128,2048]{1,0:T(8,128)(2,1)S(1)} %collective-permute-done.30.refs_2_, bf16[64,2048]{1,0:T(8,128)(2,1)S(1)} %collective-permute-done.31.refs_3_, ...), custom_call_target="tpu_custom_call" | custom-call | flops 2214592512 | bytes 10000000 | tf_op jit(solution)/shard_map/pallas_call | solution.py:37
  93.6 3.1 %collective-permute-done.12.refs_5_.refs_2_ = bf16[128,2176]{1,0:T(8,128)(2,1)S(1)} collective-permute-done((bf16[128,2176]{1,0:T(8,128)(2,1)S(1)}, bf16[128,2176]{1,0:T(8,128)(2,1)S(1)}, u32[]{:S(2)}, u32[]{:S(2)}) %collective-permute-start.12) | collective-permute-done | bytes 557088 | tf_op jit(solution)/shard_map/ppermute | solution.py:28
  103.5 2.6 %shard_map.121.refs_9_ = f32[512,1408]{1,0:T(8,128)S(1)} custom-call(bf16[128,2048]{1,0:T(8,128)(2,1)S(1)} %shard_map.120.refs_0_.normed, bf16[128,2048]{1,0:T(8,128)(2,1)S(1)} %collective-permute-done.5.refs_1_, bf16[128,2048]{1,0:T(8,128)(2,1)S(1)} %collective-permute-done.6.refs_2_, bf16[64,2048]{1,0:T(8,128)(2,1)S(1)} %collective-permute-done.7.refs_3_, ...), custom_call_target="tpu_custom_call" | custom-call | flops 2214592512 | bytes 10000000 | tf_op jit(solution)/shard_map/pallas_call | solution.py:37
  114.2 3.4 %collective-permute-done.34.left = bf16[256,512]{1,0:T(8,128)(2,1)S(1)} collective-permute-done((bf16[256,512]{1,0:T(8,128)(2,1)S(1)}, bf16[256,512]{1,0:T(8,128)(2,1)S(1)}, u32[]{:S(2)}, u32[]{:S(2)}) %collective-permute-start.34) | collective-permute-done | bytes 262176 | tf_op jit(solution)/shard_map/ppermute | solution.py:28
  117.6 2.4 %collective-permute-done.35.right = bf16[256,512]{1,0:T(8,128)(2,1)S(1)} collective-permute-done((bf16[256,512]{1,0:T(8,128)(2,1)S(1)}, bf16[256,512]{1,0:T(8,128)(2,1)S(1)}, u32[]{:S(2)}, u32[]{:S(2)}) %collective-permute-start.35) | collective-permute-done | bytes 262176 | tf_op jit(solution)/shard_map/ppermute | solution.py:28
  122.3 3.3 %collective-permute-done.40.right = bf16[256,512]{1,0:T(8,128)(2,1)S(1)} collective-permute-done((bf16[256,512]{1,0:T(8,128)(2,1)S(1)}, bf16[256,512]{1,0:T(8,128)(2,1)S(1)}, u32[]{:S(2)}, u32[]{:S(2)}) %collective-permute-start.40) | collective-permute-done | bytes 262176 | tf_op jit(solution)/shard_map/ppermute | solution.py:28
  127.9 4.1 %collective-permute-done.41.refs_4_ = bf16[128,512]{1,0:T(8,128)(2,1)S(1)} collective-permute-done((bf16[128,512]{1,0:T(8,128)(2,1)S(1)}, bf16[128,512]{1,0:T(8,128)(2,1)S(1)}, u32[]{:S(2)}, u32[]{:S(2)}) %collective-permute-start.41) | collective-permute-done | bytes 131104 | tf_op jit(solution)/shard_map/ppermute | solution.py:28
  (93 shorter events, 46.8 us)
Async XLA Ops:
  3.1 23.4 %collective-permute-start.10 = (bf16[64,2176]{1,0:T(8,128)(2,1)S(1)}, bf16[64,2176]{1,0:T(8,128)(2,1)S(1)}, u32[]{:S(2)}, u32[]{:S(2)}) collective-permute-start(bf16[64,2176]{1,0:T(8,128)(2,1)S(1)} %get-tuple-element.64), channel_id=1, source_target_pairs={{0,8},{4,12},{8,0},{12,4},{16,24},{20,28},{24,16},{28,20},{32,40},... | collective-permute-start | bytes 835592 | tf_op jit(solution)/shard_map/ppermute | solution.py:28
  20.3 29.6 %collective-permute-start.5 = (bf16[128,2048]{1,0:T(8,128)(2,1)S(1)}, bf16[128,2048]{1,0:T(8,128)(2,1)S(1)}, u32[]{:S(2)}, u32[]{:S(2)}) collective-permute-start(bf16[128,2048]{1,0:T(8,128)(2,1)S(1)} %shard_map.120.refs_0_.normed), channel_id=1, source_target_pairs={{0,1},{1,0},{2,3},{3,2},{4,5},{5,4},{6,7},{7,6},{8,9},{9,8},{10,11... | collective-permute-start | bytes 1572872 | tf_op jit(solution)/shard_map/ppermute | solution.py:28
  21.0 29.3 %collective-permute-start.6 = (bf16[128,2048]{1,0:T(8,128)(2,1)S(1)}, bf16[128,2048]{1,0:T(8,128)(2,1)S(1)}, u32[]{:S(2)}, u32[]{:S(2)}) collective-permute-start(bf16[128,2048]{1,0:T(8,128)(2,1)S(1)} %shard_map.120.refs_0_.normed), channel_id=1, source_target_pairs={{0,3},{1,2},{2,1},{3,0},{4,7},{5,6},{6,5},{7,4},{8,11},{9,10},{10,... | collective-permute-start | bytes 1572872 | tf_op jit(solution)/shard_map/ppermute | solution.py:28
  21.6 38.0 %collective-permute-start.28 = (bf16[128,2048]{1,0:T(8,128)(2,1)S(1)}, bf16[128,2048]{1,0:T(8,128)(2,1)S(1)}, u32[]{:S(2)}, u32[]{:S(2)}) collective-permute-start(bf16[128,2048]{1,0:T(8,128)(2,1)S(1)} %shard_map.120.refs_0_.normed), channel_id=1, source_target_pairs={{0,4},{4,0},{8,12},{12,8},{16,20},{20,16},{24,28},{28,24},{32,36},... | collective-permute-start | bytes 1572872 | tf_op jit(solution)/shard_map/ppermute | solution.py:28
  21.6 14.1 %collective-permute-start.13 = (bf16[64,2176]{1,0:T(8,128)(2,1)S(1)}, bf16[64,2176]{1,0:T(8,128)(2,1)S(1)}, u32[]{:S(2)}, u32[]{:S(2)}) collective-permute-start(bf16[64,2176]{1,0:T(8,128)(2,1)S(1)} %get-tuple-element.64), channel_id=1, source_target_pairs={{0,24},{4,28},{8,16},{12,20},{16,8},{20,12},{24,0},{28,4},{32,56},... | collective-permute-start | bytes 835592 | tf_op jit(solution)/shard_map/ppermute | solution.py:28
  35.1 12.4 %collective-permute-start.14 = (bf16[64,2176]{1,0:T(8,128)(2,1)S(1)}, bf16[64,2176]{1,0:T(8,128)(2,1)S(1)}, u32[]{:S(2)}, u32[]{:S(2)}) collective-permute-start(bf16[64,2176]{1,0:T(8,128)(2,1)S(1)} %get-tuple-element.64), channel_id=1, source_target_pairs={{0,16},{4,20},{8,24},{12,28},{16,0},{20,4},{24,8},{28,12},{32,48},... | collective-permute-start | bytes 835592 | tf_op jit(solution)/shard_map/ppermute | solution.py:28
  35.7 10.2 %collective-permute-start.20 = (bf16[64,2176]{1,0:T(8,128)(2,1)S(1)}, bf16[64,2176]{1,0:T(8,128)(2,1)S(1)}, u32[]{:S(2)}, u32[]{:S(2)}) collective-permute-start(bf16[64,2176]{1,0:T(8,128)(2,1)S(1)} %get-tuple-element.63), channel_id=1, source_target_pairs={{0,96},{4,100},{8,104},{12,108},{16,112},{20,116},{24,120},{28,124... | collective-permute-start | bytes 835592 | tf_op jit(solution)/shard_map/ppermute | solution.py:28
  45.9 11.0 %collective-permute-start.21 = (bf16[64,2176]{1,0:T(8,128)(2,1)S(1)}, bf16[64,2176]{1,0:T(8,128)(2,1)S(1)}, u32[]{:S(2)}, u32[]{:S(2)}) collective-permute-start(bf16[64,2176]{1,0:T(8,128)(2,1)S(1)} %get-tuple-element.63), channel_id=1, source_target_pairs={{0,64},{4,68},{8,72},{12,76},{16,80},{20,84},{24,88},{28,92},{32,9... | collective-permute-start | bytes 835592 | tf_op jit(solution)/shard_map/ppermute | solution.py:28
  47.5 21.7 %collective-permute-start.11 = (bf16[128,2176]{1,0:T(8,128)(2,1)S(1)}, bf16[128,2176]{1,0:T(8,128)(2,1)S(1)}, u32[]{:S(2)}, u32[]{:S(2)}) collective-permute-start(bf16[128,2176]{1,0:T(8,128)(2,1)S(1)} %pad_maximum_fusion.refs_5_.refs_0_), channel_id=1, source_target_pairs={{0,32},{4,36},{8,40},{12,44},{16,48},{20,52},{24,56},{28,60},{32,0... | collective-permute-start | bytes 1671176 | tf_op jit(solution)/shard_map/ppermute | solution.py:28
  49.9 19.5 %collective-permute-start.15 = (bf16[128,2176]{1,0:T(8,128)(2,1)S(1)}, bf16[128,2176]{1,0:T(8,128)(2,1)S(1)}, u32[]{:S(2)}, u32[]{:S(2)}) collective-permute-start(bf16[128,2176]{1,0:T(8,128)(2,1)S(1)} %constant_dynamic-update-slice_fusion.refs_6_.refs_1_), channel_id=1, source_target_pairs={{0,96},{4,100},{8,104},{12,108},{16,112},{20,116},{24,120},{28,124... | collective-permute-start | bytes 1671176 | tf_op jit(solution)/shard_map/ppermute | solution.py:28
  50.3 21.1 %collective-permute-start.18 = (bf16[128,2176]{1,0:T(8,128)(2,1)S(1)}, bf16[128,2176]{1,0:T(8,128)(2,1)S(1)}, u32[]{:S(2)}, u32[]{:S(2)}) collective-permute-start(bf16[128,2176]{1,0:T(8,128)(2,1)S(1)} %pad_maximum_fusion.1.refs_11_.refs_4_), channel_id=1, source_target_pairs={{0,8},{4,12},{8,0},{12,4},{16,24},{20,28},{24,16},{28,20},{32,40},... | collective-permute-start | bytes 1671176 | tf_op jit(solution)/shard_map/ppermute | solution.py:28
  64.5 15.3 %collective-permute-start.22 = (bf16[128,2176]{1,0:T(8,128)(2,1)S(1)}, bf16[128,2176]{1,0:T(8,128)(2,1)S(1)}, u32[]{:S(2)}, u32[]{:S(2)}) collective-permute-start(bf16[128,2176]{1,0:T(8,128)(2,1)S(1)} %constant_dynamic-update-slice_fusion.2.refs_12_.refs_5_), channel_id=1, source_target_pairs={{0,24},{4,28},{8,16},{12,20},{16,8},{20,12},{24,0},{28,4},{32,56},... | collective-permute-start | bytes 1671176 | tf_op jit(solution)/shard_map/ppermute | solution.py:28
  66.3 13.5 %collective-permute-start.24 = (bf16[128,2176]{1,0:T(8,128)(2,1)S(1)}, bf16[128,2176]{1,0:T(8,128)(2,1)S(1)}, u32[]{:S(2)}, u32[]{:S(2)}) collective-permute-start(bf16[128,2176]{1,0:T(8,128)(2,1)S(1)} %constant_dynamic-update-slice_fusion.refs_6_.refs_1_), channel_id=1, source_target_pairs={{0,32},{4,36},{8,40},{12,44},{16,48},{20,52},{24,56},{28,60},{32,0... | collective-permute-start | bytes 1671176 | tf_op jit(solution)/shard_map/ppermute | solution.py:28
  69.2 11.2 %collective-permute-start.25 = (bf16[128,2176]{1,0:T(8,128)(2,1)S(1)}, bf16[128,2176]{1,0:T(8,128)(2,1)S(1)}, u32[]{:S(2)}, u32[]{:S(2)}) collective-permute-start(bf16[128,2176]{1,0:T(8,128)(2,1)S(1)} %pad_maximum_fusion.refs_5_.refs_0_), channel_id=1, source_target_pairs={{0,96},{4,100},{8,104},{12,108},{16,112},{20,116},{24,120},{28,124... | collective-permute-start | bytes 1671176 | tf_op jit(solution)/shard_map/ppermute | solution.py:28
  69.4 11.1 %collective-permute-start.26 = (bf16[128,2176]{1,0:T(8,128)(2,1)S(1)}, bf16[128,2176]{1,0:T(8,128)(2,1)S(1)}, u32[]{:S(2)}, u32[]{:S(2)}) collective-permute-start(bf16[128,2176]{1,0:T(8,128)(2,1)S(1)} %constant_dynamic-update-slice_fusion.2.refs_12_.refs_5_), channel_id=1, source_target_pairs={{0,8},{4,12},{8,0},{12,4},{16,24},{20,28},{24,16},{28,20},{32,40},... | collective-permute-start | bytes 1671176 | tf_op jit(solution)/shard_map/ppermute | solution.py:28
  71.4 16.0 %collective-permute-start.27 = (bf16[128,2176]{1,0:T(8,128)(2,1)S(1)}, bf16[128,2176]{1,0:T(8,128)(2,1)S(1)}, u32[]{:S(2)}, u32[]{:S(2)}) collective-permute-start(bf16[128,2176]{1,0:T(8,128)(2,1)S(1)} %pad_maximum_fusion.1.refs_11_.refs_4_), channel_id=1, source_target_pairs={{0,24},{4,28},{8,16},{12,20},{16,8},{20,12},{24,0},{28,4},{32,56},... | collective-permute-start | bytes 1671176 | tf_op jit(solution)/shard_map/ppermute | solution.py:28
  79.8 9.5 %collective-permute-start.30 = (bf16[128,2048]{1,0:T(8,128)(2,1)S(1)}, bf16[128,2048]{1,0:T(8,128)(2,1)S(1)}, u32[]{:S(2)}, u32[]{:S(2)}) collective-permute-start(bf16[128,2048]{1,0:T(8,128)(2,1)S(1)} %collective-permute-done.6.refs_2_), channel_id=1, source_target_pairs={{0,4},{4,0},{8,12},{12,8},{16,20},{20,16},{24,28},{28,24},{32,36},... | collective-permute-start | bytes 1572872 | tf_op jit(solution)/shard_map/ppermute | solution.py:28
  80.5 16.1 %collective-permute-start.12 = (bf16[128,2176]{1,0:T(8,128)(2,1)S(1)}, bf16[128,2176]{1,0:T(8,128)(2,1)S(1)}, u32[]{:S(2)}, u32[]{:S(2)}) collective-permute-start(bf16[128,2176]{1,0:T(8,128)(2,1)S(1)} %collective-permute-done.11.refs_7_.refs_2_), channel_id=1, source_target_pairs={{0,96},{4,100},{8,104},{12,108},{16,112},{20,116},{24,120},{28,124... | collective-permute-start | bytes 1671176 | tf_op jit(solution)/shard_map/ppermute | solution.py:28
  87.3 10.2 %collective-permute-start.16 = (bf16[128,2176]{1,0:T(8,128)(2,1)S(1)}, bf16[128,2176]{1,0:T(8,128)(2,1)S(1)}, u32[]{:S(2)}, u32[]{:S(2)}) collective-permute-start(bf16[128,2176]{1,0:T(8,128)(2,1)S(1)} %collective-permute-done.15.refs_10_.refs_1_), channel_id=1, source_target_pairs={{0,32},{4,36},{8,40},{12,44},{16,48},{20,52},{24,56},{28,60},{32,0... | collective-permute-start | bytes 1671176 | tf_op jit(solution)/shard_map/ppermute | solution.py:28
  87.5 11.9 %collective-permute-start.19 = (bf16[128,2176]{1,0:T(8,128)(2,1)S(1)}, bf16[128,2176]{1,0:T(8,128)(2,1)S(1)}, u32[]{:S(2)}, u32[]{:S(2)}) collective-permute-start(bf16[128,2176]{1,0:T(8,128)(2,1)S(1)} %collective-permute-done.18.refs_13_.refs_6_), channel_id=1, source_target_pairs={{0,24},{4,28},{8,16},{12,20},{16,8},{20,12},{24,0},{28,4},{32,56},... | collective-permute-start | bytes 1671176 | tf_op jit(solution)/shard_map/ppermute | solution.py:28
  89.3 10.3 %collective-permute-start.23 = (bf16[128,2176]{1,0:T(8,128)(2,1)S(1)}, bf16[128,2176]{1,0:T(8,128)(2,1)S(1)}, u32[]{:S(2)}, u32[]{:S(2)}) collective-permute-start(bf16[128,2176]{1,0:T(8,128)(2,1)S(1)} %collective-permute-done.22.refs_16_.refs_5_), channel_id=1, source_target_pairs={{0,8},{4,12},{8,0},{12,4},{16,24},{20,28},{24,16},{28,20},{32,40},... | collective-permute-start | bytes 1671176 | tf_op jit(solution)/shard_map/ppermute | solution.py:28
  109.6 10.4 %collective-permute-start.35 = (bf16[256,512]{1,0:T(8,128)(2,1)S(1)}, bf16[256,512]{1,0:T(8,128)(2,1)S(1)}, u32[]{:S(2)}, u32[]{:S(2)}) collective-permute-start(bf16[256,512]{1,0:T(8,128)(2,1)S(1)} %get-tuple-element.49), channel_id=1, source_target_pairs={{0,3},{1,2},{2,1},{3,0},{4,7},{5,6},{6,5},{7,4},{8,11},{9,10},{10,... | collective-permute-start | bytes 786440 | tf_op jit(solution)/shard_map/ppermute | solution.py:28
  112.7 9.6 %collective-permute-start.39 = (bf16[256,512]{1,0:T(8,128)(2,1)S(1)}, bf16[256,512]{1,0:T(8,128)(2,1)S(1)}, u32[]{:S(2)}, u32[]{:S(2)}) collective-permute-start(bf16[256,512]{1,0:T(8,128)(2,1)S(1)} %get-tuple-element.56), channel_id=1, source_target_pairs={{0,1},{1,0},{2,3},{3,2},{4,5},{5,4},{6,7},{7,6},{8,9},{9,8},{10,11... | collective-permute-start | bytes 786440 | tf_op jit(solution)/shard_map/ppermute | solution.py:28
  113.6 12.0 %collective-permute-start.40 = (bf16[256,512]{1,0:T(8,128)(2,1)S(1)}, bf16[256,512]{1,0:T(8,128)(2,1)S(1)}, u32[]{:S(2)}, u32[]{:S(2)}) collective-permute-start(bf16[256,512]{1,0:T(8,128)(2,1)S(1)} %get-tuple-element.57), channel_id=1, source_target_pairs={{0,3},{1,2},{2,1},{3,0},{4,7},{5,6},{6,5},{7,4},{8,11},{9,10},{10,... | collective-permute-start | bytes 786440 | tf_op jit(solution)/shard_map/ppermute | solution.py:28
  (23 other events, 166.7 us)

commit v3 on v2

--- a/solution.py
+++ b/solution.py
@@ -198,7 +198,7 @@
 
 def down_parts(h, pieces):
     for i in range(0, len(pieces), 2):
-        p = jnp.concatenate([r[:, GU:] for r in pieces[i : i + 2]], 0)
+        p = jnp.concatenate([r[:, r.shape[1] - DN :] for r in pieces[i : i + 2]], 0)
         at = i * 128
         yield (
             at,
@@ -264,8 +264,12 @@
 def spread(low_half, high_half, axis, low):
     one = swap(low_half, axis, low), swap(high_half, axis, low)
     three = swap(low_half, axis, 3 * low), swap(high_half, axis, 3 * low)
-    two = swap(one[0], axis, 3 * low), swap(three[1], axis, low)
-    return (low_half, high_half, *one, *three, *two)
+
+    def passed_on(cols):
+        return (swap(one[0][:, cols], axis, 3 * low), swap(three[1][:, cols], axis, low))
+
+    near = (low_half, high_half, *one, *three)
+    return near, passed_on(slice(0, GU)), passed_on(slice(GU, GU + DN))
 
 
 def per_device(
@@ -312,8 +316,8 @@
         halves = (jnp.concatenate(units[i : i + 2], 0) for i in (0, 2))
         return spread(*halves, "sp", across)
 
-    all_a = columns(from_0, SP_Y, SP_Z)
-    all_b = columns(from_1, SP_Z, SP_Y)
+    near_a, gu_a, dn_a = columns(from_0, SP_Y, SP_Z)
+    near_b, gu_b, dn_b = columns(from_1, SP_Z, SP_Y)
 
     attended = call(
         attend_body,
@@ -339,27 +343,24 @@
 
     def hidden_of(r):
         early = call(
-            early_body,
-            shape((ROWS, GU), F32),
-            2 * ROWS * 1536 * GU,
-            10**7,
-            (*r, *all_a[:6], *all_b[:6]),
+            early_body, shape((ROWS, GU), F32), 2 * ROWS * 1536 * GU, 10**7, (*r, *near_a, *near_b)
         )
         return call(
             hidden_body,
             shape((ROWS, DN)),
             2 * ROWS * 512 * GU,
             10**7,
-            (*r, *all_a[6:], *all_b[6:], early),
+            (*r, *gu_a, *gu_b, early),
             (pltpu.VMEM((ROWS, GU), F32),),
         )
 
     own_hidden, other_hidden = hidden_of(rows), hidden_of(others)
     sums = []
     chunks = [slice(0, 4), slice(4, 8)]
+    all_a, all_b = (*near_a, *dn_a), (*near_b, *dn_b)
     for part_of in chunks:
         pieces = (*all_a[part_of], *all_b[part_of])
-        width = sum(p.shape[0] for p in pieces)
+        width = 128 * len(pieces)
         flops = 2 * ROWS * DN * width
         part = call(give_body, shape((ROWS, width)), flops, 10**6, (other_hidden, *pieces))
         theirs = swap(part, "sp", 1)

time: 135 us -> 137 us (1.015)
  starting transfers between devices: 51.6 us -> 59.4 us
  waiting for transfers between devices: 63 us -> 56.4 us
    ppermute x42 -> x46, starting transfers between devices: 50.9 us -> 58.8 us  [swap(): return lax.ppermute(value, axis, [(i, i ^ mask) for i in range(count)])]
    ppermute x42 -> x46, waiting for transfers between devices: 63 us -> 56.4 us  [swap(): return lax.ppermute(value, axis, [(i, i ^ mask) for i in range(count)])]
  transfers between devices with their start and end apart: 43 -> 47, of which waited for: 22 -> 19; matrix products, arithmetic and copies ran while one was open for 0% -> 0% of each run, Pallas kernels for 11% -> 12%
where the time goes in v3:
time: 137 us; the launch traced here: 136 us
  starting transfers between devices  59.4 us (43%)
  waiting for transfers between devices  56.4 us (41%)
  Pallas kernels  19.3 us (14%)
    ppermute x46, starting transfers between devices, swap(): return lax.ppermute(value, axis, [(i, i ^ mask) for i in range(count)])  58.8 us
    ppermute x46, waiting for transfers between devices, swap(): return lax.ppermute(value, axis, [(i, i ^ mask) for i in range(count)])  56.4 us
    pallas_call x14, Pallas kernels, call(): pl.pallas_call(body, out_shape=outs, in_specs=[pl.BlockSpec(memory_space=...  19.3 us
  transfers between devices with their start and end apart: 47, of which 19 were waited for; matrix products, arithmetic and copies ran while one was open for 0% of the time, Pallas kernels for 12%

profile of v3, /device:TPU:0, one launch (start us, length us, event | category | flops | bytes accessed | tf_op | source)
XLA Modules:
  0.0 135.9 jit_solution(14003565329362806292)
XLA Ops:
  3.1 2.7 %collective-permute-start.10 = (bf16[64,2176]{1,0:T(8,128)(2,1)S(1)}, bf16[64,2176]{1,0:T(8,128)(2,1)S(1)}, u32[]{:S(2)}, u32[]{:S(2)}) collective-permute-start(bf16[64,2176]{1,0:T(8,128)(2,1)S(1)} %get-tuple-element.64), channel_id=1, source_target_pairs={{0,8},{4,12},{8,0},{12,4},{16,24},{20,28},{24,16},{28,20},{32,40},... | collective-permute-start | bytes 835592 | tf_op jit(solution)/shard_map/ppermute | solution.py:28
  5.8 3.0 %shard_map.119 = (bf16[128,256]{1,0:T(8,128)(2,1)S(1)}, bf16[128,256]{1,0:T(8,128)(2,1)S(1)}, bf16[128,256]{1,0:T(8,128)(2,1)S(1)}, bf16[128,256]{1,0:T(8,128)(2,1)S(1)}) custom-call(bf16[512,256]{1,0:T(8,128)(2,1)S(1)} %get-tuple-element.34.q, bf16[512,128]{1,0:T(8,128)(2,1)S(1)} %get-tuple-element.35.k, bf16[512,128]{1,0:T(8,128)(2,1)S(1)} %get-tuple-element.36.v, ...), custom_call_target="tpu_custom_call" | custom-call | flops 1610612736 | bytes 1000000 | tf_op jit(solution)/shard_map/pallas_call | solution.py:37
  13.2 2.8 %collective-permute-done.3.a3 = bf16[128,256]{1,0:T(8,128)(2,1)S(1)} collective-permute-done((bf16[128,256]{1,0:T(8,128)(2,1)S(1)}, bf16[128,256]{1,0:T(8,128)(2,1)S(1)}, u32[]{:S(2)}, u32[]{:S(2)}) %collective-permute-start.3) | collective-permute-done | bytes 65568 | tf_op jit(solution)/shard_map/ppermute | solution.py:28
  16.0 2.7 %collective-permute-done.4.a2 = bf16[128,256]{1,0:T(8,128)(2,1)S(1)} collective-permute-done((bf16[128,256]{1,0:T(8,128)(2,1)S(1)}, bf16[128,256]{1,0:T(8,128)(2,1)S(1)}, u32[]{:S(2)}, u32[]{:S(2)}) %collective-permute-start.4) | collective-permute-done | bytes 65568 | tf_op jit(solution)/shard_map/ppermute | solution.py:28
  21.6 4.9 %collective-permute-start.13 = (bf16[64,2176]{1,0:T(8,128)(2,1)S(1)}, bf16[64,2176]{1,0:T(8,128)(2,1)S(1)}, u32[]{:S(2)}, u32[]{:S(2)}) collective-permute-start(bf16[64,2176]{1,0:T(8,128)(2,1)S(1)} %get-tuple-element.64), channel_id=1, source_target_pairs={{0,24},{4,28},{8,16},{12,20},{16,8},{20,12},{24,0},{28,4},{32,56},... | collective-permute-start | bytes 835592 | tf_op jit(solution)/shard_map/ppermute | solution.py:28
  28.5 6.7 %collective-permute-done.17 = bf16[64,2176]{1,0:T(8,128)(2,1)S(1)} collective-permute-done((bf16[64,2176]{1,0:T(8,128)(2,1)S(1)}, bf16[64,2176]{1,0:T(8,128)(2,1)S(1)}, u32[]{:S(2)}, u32[]{:S(2)}) %collective-permute-start.17) | collective-permute-done | bytes 278560 | tf_op jit(solution)/shard_map/ppermute | solution.py:28
  35.7 3.9 %collective-permute-start.20 = (bf16[64,2176]{1,0:T(8,128)(2,1)S(1)}, bf16[64,2176]{1,0:T(8,128)(2,1)S(1)}, u32[]{:S(2)}, u32[]{:S(2)}) collective-permute-start(bf16[64,2176]{1,0:T(8,128)(2,1)S(1)} %get-tuple-element.63), channel_id=1, source_target_pairs={{0,96},{4,100},{8,104},{12,108},{16,112},{20,116},{24,120},{28,124... | collective-permute-start | bytes 835592 | tf_op jit(solution)/shard_map/ppermute | solution.py:28
  39.7 6.3 %collective-permute-done.20 = bf16[64,2176]{1,0:T(8,128)(2,1)S(1)} collective-permute-done((bf16[64,2176]{1,0:T(8,128)(2,1)S(1)}, bf16[64,2176]{1,0:T(8,128)(2,1)S(1)}, u32[]{:S(2)}, u32[]{:S(2)}) %collective-permute-start.20) | collective-permute-done | bytes 278560 | tf_op jit(solution)/shard_map/ppermute | solution.py:28
  47.5 2.3 %collective-permute-start.11 = (bf16[128,2176]{1,0:T(8,128)(2,1)S(1)}, bf16[128,2176]{1,0:T(8,128)(2,1)S(1)}, u32[]{:S(2)}, u32[]{:S(2)}) collective-permute-start(bf16[128,2176]{1,0:T(8,128)(2,1)S(1)} %pad_maximum_fusion.refs_5_.refs_0_), channel_id=1, source_target_pairs={{0,32},{4,36},{8,40},{12,44},{16,48},{20,52},{24,56},{28,60},{32,0... | collective-permute-start | bytes 1671176 | tf_op jit(solution)/shard_map/ppermute | solution.py:28
  52.6 4.4 %collective-permute-done.21 = bf16[64,2176]{1,0:T(8,128)(2,1)S(1)} collective-permute-done((bf16[64,2176]{1,0:T(8,128)(2,1)S(1)}, bf16[64,2176]{1,0:T(8,128)(2,1)S(1)}, u32[]{:S(2)}, u32[]{:S(2)}) %collective-permute-start.21) | collective-permute-done | bytes 278560 | tf_op jit(solution)/shard_map/ppermute | solution.py:28
  57.0 2.6 %collective-permute-start.7 = (bf16[64,2048]{1,0:T(8,128)(2,1)S(1)}, bf16[64,2048]{1,0:T(8,128)(2,1)S(1)}, u32[]{:S(2)}, u32[]{:S(2)}) collective-permute-start(bf16[64,2048]{1,0:T(8,128)(2,1)S(1)} %slice.40), channel_id=1, source_target_pairs={{0,3},{1,2},{2,1},{3,0},{4,7},{5,6},{6,5},{7,4},{8,11},{9,10},{10,... | collective-permute-start | bytes 786440 | tf_op jit(solution)/shard_map/ppermute | solution.py:28
  59.8 4.7 %collective-permute-done.7.refs_3_ = bf16[64,2048]{1,0:T(8,128)(2,1)S(1)} collective-permute-done((bf16[64,2048]{1,0:T(8,128)(2,1)S(1)}, bf16[64,2048]{1,0:T(8,128)(2,1)S(1)}, u32[]{:S(2)}, u32[]{:S(2)}) %collective-permute-start.7) | collective-permute-done | bytes 262176 | tf_op jit(solution)/shard_map/ppermute | solution.py:28
  66.7 2.6 %collective-permute-done.11.refs_7_.refs_2_ = bf16[128,2176]{1,0:T(8,128)(2,1)S(1)} collective-permute-done((bf16[128,2176]{1,0:T(8,128)(2,1)S(1)}, bf16[128,2176]{1,0:T(8,128)(2,1)S(1)}, u32[]{:S(2)}, u32[]{:S(2)}) %collective-permute-start.11) | collective-permute-done | bytes 557088 | tf_op jit(solution)/shard_map/ppermute | solution.py:28
  72.4 7.4 %collective-permute-done.22.refs_16_.refs_5_ = bf16[128,2176]{1,0:T(8,128)(2,1)S(1)} collective-permute-done((bf16[128,2176]{1,0:T(8,128)(2,1)S(1)}, bf16[128,2176]{1,0:T(8,128)(2,1)S(1)}, u32[]{:S(2)}, u32[]{:S(2)}) %collective-permute-start.22) | collective-permute-done | bytes 557088 | tf_op jit(solution)/shard_map/ppermute | solution.py:28
  80.5 3.5 %collective-permute-start.12 = (bf16[128,1408]{1,0:T(8,128)(2,1)S(1)}, bf16[128,1408]{1,0:T(8,128)(2,1)S(1)}, u32[]{:S(2)}, u32[]{:S(2)}) collective-permute-start(bf16[128,1408]{1,0:T(8,128)(2,1)S(1)} %slice.42), channel_id=1, source_target_pairs={{0,96},{4,100},{8,104},{12,108},{16,112},{20,116},{24,120},{28,124... | collective-permute-start | bytes 1081352 | tf_op jit(solution)/shard_map/ppermute | solution.py:28
  84.0 3.3 %collective-permute-done.27.refs_15_.refs_4_ = bf16[128,2176]{1,0:T(8,128)(2,1)S(1)} collective-permute-done((bf16[128,2176]{1,0:T(8,128)(2,1)S(1)}, bf16[128,2176]{1,0:T(8,128)(2,1)S(1)}, u32[]{:S(2)}, u32[]{:S(2)}) %collective-permute-start.27) | collective-permute-done | bytes 557088 | tf_op jit(solution)/shard_map/ppermute | solution.py:28
  90.9 3.2 %collective-permute-start.38 = (bf16[128,768]{1,0:T(8,128)(2,1)S(1)}, bf16[128,768]{1,0:T(8,128)(2,1)S(1)}, u32[]{:S(2)}, u32[]{:S(2)}) collective-permute-start(bf16[128,768]{1,0:T(8,128)(2,1)S(1)} %slice.46), channel_id=1, source_target_pairs={{0,96},{4,100},{8,104},{12,108},{16,112},{20,116},{24,120},{28,124... | collective-permute-start | bytes 589832 | tf_op jit(solution)/shard_map/ppermute | solution.py:28
  98.1 2.6 %shard_map.123.refs_9_ = f32[512,1408]{1,0:T(8,128)S(1)} custom-call(bf16[128,2048]{1,0:T(8,128)(2,1)S(1)} %collective-permute-done.28.refs_0_, bf16[128,2048]{1,0:T(8,128)(2,1)S(1)} %collective-permute-done.29.refs_1_, bf16[128,2048]{1,0:T(8,128)(2,1)S(1)} %collective-permute-done.30.refs_2_, bf16[64,2048]{1,0:T(8,128)(2,1)S(1)} %collective-permute-done.31.refs_3_, ...), custom_call_target="tpu_custom_call" | custom-call | flops 2214592512 | bytes 10000000 | tf_op jit(solution)/shard_map/pallas_call | solution.py:37
  105.6 2.6 %shard_map.121.refs_9_ = f32[512,1408]{1,0:T(8,128)S(1)} custom-call(bf16[128,2048]{1,0:T(8,128)(2,1)S(1)} %shard_map.120.refs_0_.normed, bf16[128,2048]{1,0:T(8,128)(2,1)S(1)} %collective-permute-done.5.refs_1_, bf16[128,2048]{1,0:T(8,128)(2,1)S(1)} %collective-permute-done.6.refs_2_, bf16[64,2048]{1,0:T(8,128)(2,1)S(1)} %collective-permute-done.7.refs_3_, ...), custom_call_target="tpu_custom_call" | custom-call | flops 2214592512 | bytes 10000000 | tf_op jit(solution)/shard_map/pallas_call | solution.py:37
  110.7 2.6 %collective-permute-start.35 = (bf16[256,512]{1,0:T(8,128)(2,1)S(1)}, bf16[256,512]{1,0:T(8,128)(2,1)S(1)}, u32[]{:S(2)}, u32[]{:S(2)}) collective-permute-start(bf16[256,512]{1,0:T(8,128)(2,1)S(1)} %get-tuple-element.49), channel_id=1, source_target_pairs={{0,3},{1,2},{2,1},{3,0},{4,7},{5,6},{6,5},{7,4},{8,11},{9,10},{10,... | collective-permute-start | bytes 786440 | tf_op jit(solution)/shard_map/ppermute | solution.py:28
  116.3 3.4 %collective-permute-done.34.left = bf16[256,512]{1,0:T(8,128)(2,1)S(1)} collective-permute-done((bf16[256,512]{1,0:T(8,128)(2,1)S(1)}, bf16[256,512]{1,0:T(8,128)(2,1)S(1)}, u32[]{:S(2)}, u32[]{:S(2)}) %collective-permute-start.34) | collective-permute-done | bytes 262176 | tf_op jit(solution)/shard_map/ppermute | solution.py:28
  121.2 2.6 %collective-permute-start.36 = (bf16[128,512]{1,0:T(8,128)(2,1)S(1)}, bf16[128,512]{1,0:T(8,128)(2,1)S(1)}, u32[]{:S(2)}, u32[]{:S(2)}) collective-permute-start(bf16[128,512]{1,0:T(8,128)(2,1)S(1)} %get-tuple-element.53), channel_id=1, source_target_pairs={{0,3},{1,2},{2,1},{3,0},{4,7},{5,6},{6,5},{7,4},{8,11},{9,10},{10,... | collective-permute-start | bytes 393224 | tf_op jit(solution)/shard_map/ppermute | solution.py:28
  126.8 2.6 %collective-permute-start.45 = (bf16[128,512]{1,0:T(8,128)(2,1)S(1)}, bf16[128,512]{1,0:T(8,128)(2,1)S(1)}, u32[]{:S(2)}, u32[]{:S(2)}) collective-permute-start(bf16[128,512]{1,0:T(8,128)(2,1)S(1)} %get-tuple-element.61), channel_id=1, source_target_pairs={{0,3},{1,2},{2,1},{3,0},{4,7},{5,6},{6,5},{7,4},{8,11},{9,10},{10,... | collective-permute-start | bytes 393224 | tf_op jit(solution)/shard_map/ppermute | solution.py:28
  129.5 3.5 %collective-permute-done.45.refs_4_ = bf16[128,512]{1,0:T(8,128)(2,1)S(1)} collective-permute-done((bf16[128,512]{1,0:T(8,128)(2,1)S(1)}, bf16[128,512]{1,0:T(8,128)(2,1)S(1)}, u32[]{:S(2)}, u32[]{:S(2)}) %collective-permute-start.45) | collective-permute-done | bytes 131104 | tf_op jit(solution)/shard_map/ppermute | solution.py:28
  (109 shorter events, 48.8 us)
Async XLA Ops:
  3.1 23.4 %collective-permute-start.10 = (bf16[64,2176]{1,0:T(8,128)(2,1)S(1)}, bf16[64,2176]{1,0:T(8,128)(2,1)S(1)}, u32[]{:S(2)}, u32[]{:S(2)}) collective-permute-start(bf16[64,2176]{1,0:T(8,128)(2,1)S(1)} %get-tuple-element.64), channel_id=1, source_target_pairs={{0,8},{4,12},{8,0},{12,4},{16,24},{20,28},{24,16},{28,20},{32,40},... | collective-permute-start | bytes 835592 | tf_op jit(solution)/shard_map/ppermute | solution.py:28
  20.3 29.6 %collective-permute-start.5 = (bf16[128,2048]{1,0:T(8,128)(2,1)S(1)}, bf16[128,2048]{1,0:T(8,128)(2,1)S(1)}, u32[]{:S(2)}, u32[]{:S(2)}) collective-permute-start(bf16[128,2048]{1,0:T(8,128)(2,1)S(1)} %shard_map.120.refs_0_.normed), channel_id=1, source_target_pairs={{0,1},{1,0},{2,3},{3,2},{4,5},{5,4},{6,7},{7,6},{8,9},{9,8},{10,11... | collective-permute-start | bytes 1572872 | tf_op jit(solution)/shard_map/ppermute | solution.py:28
  21.0 29.3 %collective-permute-start.6 = (bf16[128,2048]{1,0:T(8,128)(2,1)S(1)}, bf16[128,2048]{1,0:T(8,128)(2,1)S(1)}, u32[]{:S(2)}, u32[]{:S(2)}) collective-permute-start(bf16[128,2048]{1,0:T(8,128)(2,1)S(1)} %shard_map.120.refs_0_.normed), channel_id=1, source_target_pairs={{0,3},{1,2},{2,1},{3,0},{4,7},{5,6},{6,5},{7,4},{8,11},{9,10},{10,... | collective-permute-start | bytes 1572872 | tf_op jit(solution)/shard_map/ppermute | solution.py:28
  21.6 38.0 %collective-permute-start.28 = (bf16[128,2048]{1,0:T(8,128)(2,1)S(1)}, bf16[128,2048]{1,0:T(8,128)(2,1)S(1)}, u32[]{:S(2)}, u32[]{:S(2)}) collective-permute-start(bf16[128,2048]{1,0:T(8,128)(2,1)S(1)} %shard_map.120.refs_0_.normed), channel_id=1, source_target_pairs={{0,4},{4,0},{8,12},{12,8},{16,20},{20,16},{24,28},{28,24},{32,36},... | collective-permute-start | bytes 1572872 | tf_op jit(solution)/shard_map/ppermute | solution.py:28
  21.6 14.1 %collective-permute-start.13 = (bf16[64,2176]{1,0:T(8,128)(2,1)S(1)}, bf16[64,2176]{1,0:T(8,128)(2,1)S(1)}, u32[]{:S(2)}, u32[]{:S(2)}) collective-permute-start(bf16[64,2176]{1,0:T(8,128)(2,1)S(1)} %get-tuple-element.64), channel_id=1, source_target_pairs={{0,24},{4,28},{8,16},{12,20},{16,8},{20,12},{24,0},{28,4},{32,56},... | collective-permute-start | bytes 835592 | tf_op jit(solution)/shard_map/ppermute | solution.py:28
  35.1 12.4 %collective-permute-start.14 = (bf16[64,2176]{1,0:T(8,128)(2,1)S(1)}, bf16[64,2176]{1,0:T(8,128)(2,1)S(1)}, u32[]{:S(2)}, u32[]{:S(2)}) collective-permute-start(bf16[64,2176]{1,0:T(8,128)(2,1)S(1)} %get-tuple-element.64), channel_id=1, source_target_pairs={{0,16},{4,20},{8,24},{12,28},{16,0},{20,4},{24,8},{28,12},{32,48},... | collective-permute-start | bytes 835592 | tf_op jit(solution)/shard_map/ppermute | solution.py:28
  35.7 10.2 %collective-permute-start.20 = (bf16[64,2176]{1,0:T(8,128)(2,1)S(1)}, bf16[64,2176]{1,0:T(8,128)(2,1)S(1)}, u32[]{:S(2)}, u32[]{:S(2)}) collective-permute-start(bf16[64,2176]{1,0:T(8,128)(2,1)S(1)} %get-tuple-element.63), channel_id=1, source_target_pairs={{0,96},{4,100},{8,104},{12,108},{16,112},{20,116},{24,120},{28,124... | collective-permute-start | bytes 835592 | tf_op jit(solution)/shard_map/ppermute | solution.py:28
  45.9 11.0 %collective-permute-start.21 = (bf16[64,2176]{1,0:T(8,128)(2,1)S(1)}, bf16[64,2176]{1,0:T(8,128)(2,1)S(1)}, u32[]{:S(2)}, u32[]{:S(2)}) collective-permute-start(bf16[64,2176]{1,0:T(8,128)(2,1)S(1)} %get-tuple-element.63), channel_id=1, source_target_pairs={{0,64},{4,68},{8,72},{12,76},{16,80},{20,84},{24,88},{28,92},{32,9... | collective-permute-start | bytes 835592 | tf_op jit(solution)/shard_map/ppermute | solution.py:28
  47.5 21.7 %collective-permute-start.11 = (bf16[128,2176]{1,0:T(8,128)(2,1)S(1)}, bf16[128,2176]{1,0:T(8,128)(2,1)S(1)}, u32[]{:S(2)}, u32[]{:S(2)}) collective-permute-start(bf16[128,2176]{1,0:T(8,128)(2,1)S(1)} %pad_maximum_fusion.refs_5_.refs_0_), channel_id=1, source_target_pairs={{0,32},{4,36},{8,40},{12,44},{16,48},{20,52},{24,56},{28,60},{32,0... | collective-permute-start | bytes 1671176 | tf_op jit(solution)/shard_map/ppermute | solution.py:28
  49.9 19.5 %collective-permute-start.15 = (bf16[128,2176]{1,0:T(8,128)(2,1)S(1)}, bf16[128,2176]{1,0:T(8,128)(2,1)S(1)}, u32[]{:S(2)}, u32[]{:S(2)}) collective-permute-start(bf16[128,2176]{1,0:T(8,128)(2,1)S(1)} %constant_dynamic-update-slice_fusion.refs_6_.refs_1_), channel_id=1, source_target_pairs={{0,96},{4,100},{8,104},{12,108},{16,112},{20,116},{24,120},{28,124... | collective-permute-start | bytes 1671176 | tf_op jit(solution)/shard_map/ppermute | solution.py:28
  50.3 21.1 %collective-permute-start.18 = (bf16[128,2176]{1,0:T(8,128)(2,1)S(1)}, bf16[128,2176]{1,0:T(8,128)(2,1)S(1)}, u32[]{:S(2)}, u32[]{:S(2)}) collective-permute-start(bf16[128,2176]{1,0:T(8,128)(2,1)S(1)} %pad_maximum_fusion.1.refs_11_.refs_4_), channel_id=1, source_target_pairs={{0,8},{4,12},{8,0},{12,4},{16,24},{20,28},{24,16},{28,20},{32,40},... | collective-permute-start | bytes 1671176 | tf_op jit(solution)/shard_map/ppermute | solution.py:28
  64.5 15.3 %collective-permute-start.22 = (bf16[128,2176]{1,0:T(8,128)(2,1)S(1)}, bf16[128,2176]{1,0:T(8,128)(2,1)S(1)}, u32[]{:S(2)}, u32[]{:S(2)}) collective-permute-start(bf16[128,2176]{1,0:T(8,128)(2,1)S(1)} %constant_dynamic-update-slice_fusion.2.refs_12_.refs_5_), channel_id=1, source_target_pairs={{0,24},{4,28},{8,16},{12,20},{16,8},{20,12},{24,0},{28,4},{32,56},... | collective-permute-start | bytes 1671176 | tf_op jit(solution)/shard_map/ppermute | solution.py:28
  66.3 13.5 %collective-permute-start.24 = (bf16[128,2176]{1,0:T(8,128)(2,1)S(1)}, bf16[128,2176]{1,0:T(8,128)(2,1)S(1)}, u32[]{:S(2)}, u32[]{:S(2)}) collective-permute-start(bf16[128,2176]{1,0:T(8,128)(2,1)S(1)} %constant_dynamic-update-slice_fusion.refs_6_.refs_1_), channel_id=1, source_target_pairs={{0,32},{4,36},{8,40},{12,44},{16,48},{20,52},{24,56},{28,60},{32,0... | collective-permute-start | bytes 1671176 | tf_op jit(solution)/shard_map/ppermute | solution.py:28
  69.2 11.2 %collective-permute-start.25 = (bf16[128,2176]{1,0:T(8,128)(2,1)S(1)}, bf16[128,2176]{1,0:T(8,128)(2,1)S(1)}, u32[]{:S(2)}, u32[]{:S(2)}) collective-permute-start(bf16[128,2176]{1,0:T(8,128)(2,1)S(1)} %pad_maximum_fusion.refs_5_.refs_0_), channel_id=1, source_target_pairs={{0,96},{4,100},{8,104},{12,108},{16,112},{20,116},{24,120},{28,124... | collective-permute-start | bytes 1671176 | tf_op jit(solution)/shard_map/ppermute | solution.py:28
  69.4 11.1 %collective-permute-start.26 = (bf16[128,2176]{1,0:T(8,128)(2,1)S(1)}, bf16[128,2176]{1,0:T(8,128)(2,1)S(1)}, u32[]{:S(2)}, u32[]{:S(2)}) collective-permute-start(bf16[128,2176]{1,0:T(8,128)(2,1)S(1)} %constant_dynamic-update-slice_fusion.2.refs_12_.refs_5_), channel_id=1, source_target_pairs={{0,8},{4,12},{8,0},{12,4},{16,24},{20,28},{24,16},{28,20},{32,40},... | collective-permute-start | bytes 1671176 | tf_op jit(solution)/shard_map/ppermute | solution.py:28
  71.4 16.0 %collective-permute-start.27 = (bf16[128,2176]{1,0:T(8,128)(2,1)S(1)}, bf16[128,2176]{1,0:T(8,128)(2,1)S(1)}, u32[]{:S(2)}, u32[]{:S(2)}) collective-permute-start(bf16[128,2176]{1,0:T(8,128)(2,1)S(1)} %pad_maximum_fusion.1.refs_11_.refs_4_), channel_id=1, source_target_pairs={{0,24},{4,28},{8,16},{12,20},{16,8},{20,12},{24,0},{28,4},{32,56},... | collective-permute-start | bytes 1671176 | tf_op jit(solution)/shard_map/ppermute | solution.py:28
  79.8 9.5 %collective-permute-start.30 = (bf16[128,2048]{1,0:T(8,128)(2,1)S(1)}, bf16[128,2048]{1,0:T(8,128)(2,1)S(1)}, u32[]{:S(2)}, u32[]{:S(2)}) collective-permute-start(bf16[128,2048]{1,0:T(8,128)(2,1)S(1)} %collective-permute-done.6.refs_2_), channel_id=1, source_target_pairs={{0,4},{4,0},{8,12},{12,8},{16,20},{20,16},{24,28},{28,24},{32,36},... | collective-permute-start | bytes 1572872 | tf_op jit(solution)/shard_map/ppermute | solution.py:28
  80.5 13.6 %collective-permute-start.12 = (bf16[128,1408]{1,0:T(8,128)(2,1)S(1)}, bf16[128,1408]{1,0:T(8,128)(2,1)S(1)}, u32[]{:S(2)}, u32[]{:S(2)}) collective-permute-start(bf16[128,1408]{1,0:T(8,128)(2,1)S(1)} %slice.42), channel_id=1, source_target_pairs={{0,96},{4,100},{8,104},{12,108},{16,112},{20,116},{24,120},{28,124... | collective-permute-start | bytes 1081352 | tf_op jit(solution)/shard_map/ppermute | solution.py:28
  87.5 9.9 %collective-permute-start.19 = (bf16[128,1408]{1,0:T(8,128)(2,1)S(1)}, bf16[128,1408]{1,0:T(8,128)(2,1)S(1)}, u32[]{:S(2)}, u32[]{:S(2)}) collective-permute-start(bf16[128,1408]{1,0:T(8,128)(2,1)S(1)} %slice.44), channel_id=1, source_target_pairs={{0,24},{4,28},{8,16},{12,20},{16,8},{20,12},{24,0},{28,4},{32,56},... | collective-permute-start | bytes 1081352 | tf_op jit(solution)/shard_map/ppermute | solution.py:28
  89.4 11.4 %collective-permute-start.23 = (bf16[128,1408]{1,0:T(8,128)(2,1)S(1)}, bf16[128,1408]{1,0:T(8,128)(2,1)S(1)}, u32[]{:S(2)}, u32[]{:S(2)}) collective-permute-start(bf16[128,1408]{1,0:T(8,128)(2,1)S(1)} %slice.45), channel_id=1, source_target_pairs={{0,8},{4,12},{8,0},{12,4},{16,24},{20,28},{24,16},{28,20},{32,40},... | collective-permute-start | bytes 1081352 | tf_op jit(solution)/shard_map/ppermute | solution.py:28
  90.9 12.2 %collective-permute-start.38 = (bf16[128,768]{1,0:T(8,128)(2,1)S(1)}, bf16[128,768]{1,0:T(8,128)(2,1)S(1)}, u32[]{:S(2)}, u32[]{:S(2)}) collective-permute-start(bf16[128,768]{1,0:T(8,128)(2,1)S(1)} %slice.46), channel_id=1, source_target_pairs={{0,96},{4,100},{8,104},{12,108},{16,112},{20,116},{24,120},{28,124... | collective-permute-start | bytes 589832 | tf_op jit(solution)/shard_map/ppermute | solution.py:28
  110.7 10.4 %collective-permute-start.35 = (bf16[256,512]{1,0:T(8,128)(2,1)S(1)}, bf16[256,512]{1,0:T(8,128)(2,1)S(1)}, u32[]{:S(2)}, u32[]{:S(2)}) collective-permute-start(bf16[256,512]{1,0:T(8,128)(2,1)S(1)} %get-tuple-element.49), channel_id=1, source_target_pairs={{0,3},{1,2},{2,1},{3,0},{4,7},{5,6},{6,5},{7,4},{8,11},{9,10},{10,... | collective-permute-start | bytes 786440 | tf_op jit(solution)/shard_map/ppermute | solution.py:28
  114.3 10.6 %collective-permute-start.43 = (bf16[256,512]{1,0:T(8,128)(2,1)S(1)}, bf16[256,512]{1,0:T(8,128)(2,1)S(1)}, u32[]{:S(2)}, u32[]{:S(2)}) collective-permute-start(bf16[256,512]{1,0:T(8,128)(2,1)S(1)} %get-tuple-element.56), channel_id=1, source_target_pairs={{0,1},{1,0},{2,3},{3,2},{4,5},{5,4},{6,7},{7,6},{8,9},{9,8},{10,11... | collective-permute-start | bytes 786440 | tf_op jit(solution)/shard_map/ppermute | solution.py:28
  115.7 11.0 %collective-permute-start.44 = (bf16[256,512]{1,0:T(8,128)(2,1)S(1)}, bf16[256,512]{1,0:T(8,128)(2,1)S(1)}, u32[]{:S(2)}, u32[]{:S(2)}) collective-permute-start(bf16[256,512]{1,0:T(8,128)(2,1)S(1)} %get-tuple-element.57), channel_id=1, source_target_pairs={{0,3},{1,2},{2,1},{3,0},{4,7},{5,6},{6,5},{7,4},{8,11},{9,10},{10,... | collective-permute-start | bytes 786440 | tf_op jit(solution)/shard_map/ppermute | solution.py:28
  (27 other events, 199.6 us)

commit v4 on v3

--- a/solution.py
+++ b/solution.py
@@ -213,6 +213,12 @@
         out[:, a:b] = v.astype(BF)
 
 
+def hidden_give_body(*refs):
+    inputs, pieces, (out, part, acc) = refs[:10], refs[10:-3], refs[-3:]
+    hidden_body(*inputs, out, acc)
+    give_body(out, *pieces, part)
+
+
 def take_body(h, theirs, *refs):
     pieces, (own, left, right, left_keep, right_keep) = refs[:-5], refs[-5:]
     half = own.shape[1] // 2
@@ -341,28 +347,32 @@
     rows = (normed, x1, x3, swap(x1[:mid], "tp", 3), swap(x3[mid:], "tp", 1))
     others = [swap(r, "sp", 1) for r in rows]
 
-    def hidden_of(r):
+    def hidden_of(i, r):
         early = call(
             early_body, shape((ROWS, GU), F32), 2 * ROWS * 1536 * GU, 10**7, (*r, *near_a, *near_b)
         )
+        first = (*near_a[:4], *near_b[:4]) if i else ()
         return call(
-            hidden_body,
-            shape((ROWS, DN)),
+            hidden_give_body if i else hidden_body,
+            (shape((ROWS, DN)), shape((ROWS, 1024))) if i else shape((ROWS, DN)),
             2 * ROWS * 512 * GU,
             10**7,
-            (*r, *gu_a, *gu_b, early),
+            (*r, *gu_a, *gu_b, early, *first),
             (pltpu.VMEM((ROWS, GU), F32),),
         )
 
-    own_hidden, other_hidden = hidden_of(rows), hidden_of(others)
+    own_hidden = hidden_of(0, rows)
+    other_hidden, part = hidden_of(1, others)
     sums = []
     chunks = [slice(0, 4), slice(4, 8)]
     all_a, all_b = (*near_a, *dn_a), (*near_b, *dn_b)
-    for part_of in chunks:
+    for n, part_of in enumerate(chunks):
         pieces = (*all_a[part_of], *all_b[part_of])
         width = 128 * len(pieces)
         flops = 2 * ROWS * DN * width
-        part = call(give_body, shape((ROWS, width)), flops, 10**6, (other_hidden, *pieces))
+        if n:
+            args = (other_hidden, *pieces)
+            part = call(give_body, shape((ROWS, width)), flops, 10**6, args)
         theirs = swap(part, "sp", 1)
         half = width // 2
         own, left, right, *keeps = call(

time: 137 us -> 137 us (level)
    pallas_call x14 -> x13, Pallas kernels: 19.3 us -> 19 us  [call(): pl.pallas_call(body, out_shape=outs, in_specs=[pl.BlockSpec(memory_space=...]
  transfers between devices with their start and end apart: 47 -> 47, of which waited for: 19 -> 20; matrix products, arithmetic and copies ran while one was open for 0% -> 0% of each run, Pallas kernels for 12% -> 12%
where the time goes in v4:
time: 137 us; the launch traced here: 136 us
  starting transfers between devices  59.4 us (43%)
  waiting for transfers between devices  56.7 us (41%)
  Pallas kernels  19 us (14%)
    ppermute x46, starting transfers between devices, swap(): return lax.ppermute(value, axis, [(i, i ^ mask) for i in range(count)])  58.8 us
    ppermute x46, waiting for transfers between devices, swap(): return lax.ppermute(value, axis, [(i, i ^ mask) for i in range(count)])  56.7 us
    pallas_call x13, Pallas kernels, call(): pl.pallas_call(body, out_shape=outs, in_specs=[pl.BlockSpec(memory_space=...  19 us
  transfers between devices with their start and end apart: 47, of which 20 were waited for; matrix products, arithmetic and copies ran while one was open for 0% of the time, Pallas kernels for 12%

profile of v4, /device:TPU:0, one launch (start us, length us, event | category | flops | bytes accessed | tf_op | source)
XLA Modules:
  0.0 136.0 jit_solution(220282502734277341)
XLA Ops:
  3.1 2.7 %collective-permute-start.10 = (bf16[64,2176]{1,0:T(8,128)(2,1)S(1)}, bf16[64,2176]{1,0:T(8,128)(2,1)S(1)}, u32[]{:S(2)}, u32[]{:S(2)}) collective-permute-start(bf16[64,2176]{1,0:T(8,128)(2,1)S(1)} %get-tuple-element.68), channel_id=1, source_target_pairs={{0,8},{4,12},{8,0},{12,4},{16,24},{20,28},{24,16},{28,20},{32,40},... | collective-permute-start | bytes 835592 | tf_op jit(solution)/shard_map/ppermute | solution.py:28
  5.8 3.0 %shard_map.119 = (bf16[128,256]{1,0:T(8,128)(2,1)S(1)}, bf16[128,256]{1,0:T(8,128)(2,1)S(1)}, bf16[128,256]{1,0:T(8,128)(2,1)S(1)}, bf16[128,256]{1,0:T(8,128)(2,1)S(1)}) custom-call(bf16[512,256]{1,0:T(8,128)(2,1)S(1)} %get-tuple-element.36.q, bf16[512,128]{1,0:T(8,128)(2,1)S(1)} %get-tuple-element.37.k, bf16[512,128]{1,0:T(8,128)(2,1)S(1)} %get-tuple-element.38.v, ...), custom_call_target="tpu_custom_call" | custom-call | flops 1610612736 | bytes 1000000 | tf_op jit(solution)/shard_map/pallas_call | solution.py:37
  13.2 2.8 %collective-permute-done.3.a3 = bf16[128,256]{1,0:T(8,128)(2,1)S(1)} collective-permute-done((bf16[128,256]{1,0:T(8,128)(2,1)S(1)}, bf16[128,256]{1,0:T(8,128)(2,1)S(1)}, u32[]{:S(2)}, u32[]{:S(2)}) %collective-permute-start.3) | collective-permute-done | bytes 65568 | tf_op jit(solution)/shard_map/ppermute | solution.py:28
  16.0 2.7 %collective-permute-done.4.a2 = bf16[128,256]{1,0:T(8,128)(2,1)S(1)} collective-permute-done((bf16[128,256]{1,0:T(8,128)(2,1)S(1)}, bf16[128,256]{1,0:T(8,128)(2,1)S(1)}, u32[]{:S(2)}, u32[]{:S(2)}) %collective-permute-start.4) | collective-permute-done | bytes 65568 | tf_op jit(solution)/shard_map/ppermute | solution.py:28
  21.6 4.9 %collective-permute-start.13 = (bf16[64,2176]{1,0:T(8,128)(2,1)S(1)}, bf16[64,2176]{1,0:T(8,128)(2,1)S(1)}, u32[]{:S(2)}, u32[]{:S(2)}) collective-permute-start(bf16[64,2176]{1,0:T(8,128)(2,1)S(1)} %get-tuple-element.68), channel_id=1, source_target_pairs={{0,24},{4,28},{8,16},{12,20},{16,8},{20,12},{24,0},{28,4},{32,56},... | collective-permute-start | bytes 835592 | tf_op jit(solution)/shard_map/ppermute | solution.py:28
  28.5 6.7 %collective-permute-done.17 = bf16[64,2176]{1,0:T(8,128)(2,1)S(1)} collective-permute-done((bf16[64,2176]{1,0:T(8,128)(2,1)S(1)}, bf16[64,2176]{1,0:T(8,128)(2,1)S(1)}, u32[]{:S(2)}, u32[]{:S(2)}) %collective-permute-start.17) | collective-permute-done | bytes 278560 | tf_op jit(solution)/shard_map/ppermute | solution.py:28
  35.7 3.9 %collective-permute-start.20 = (bf16[64,2176]{1,0:T(8,128)(2,1)S(1)}, bf16[64,2176]{1,0:T(8,128)(2,1)S(1)}, u32[]{:S(2)}, u32[]{:S(2)}) collective-permute-start(bf16[64,2176]{1,0:T(8,128)(2,1)S(1)} %get-tuple-element.67), channel_id=1, source_target_pairs={{0,96},{4,100},{8,104},{12,108},{16,112},{20,116},{24,120},{28,124... | collective-permute-start | bytes 835592 | tf_op jit(solution)/shard_map/ppermute | solution.py:28
  39.6 6.3 %collective-permute-done.20 = bf16[64,2176]{1,0:T(8,128)(2,1)S(1)} collective-permute-done((bf16[64,2176]{1,0:T(8,128)(2,1)S(1)}, bf16[64,2176]{1,0:T(8,128)(2,1)S(1)}, u32[]{:S(2)}, u32[]{:S(2)}) %collective-permute-start.20) | collective-permute-done | bytes 278560 | tf_op jit(solution)/shard_map/ppermute | solution.py:28
  47.5 2.3 %collective-permute-start.11 = (bf16[128,2176]{1,0:T(8,128)(2,1)S(1)}, bf16[128,2176]{1,0:T(8,128)(2,1)S(1)}, u32[]{:S(2)}, u32[]{:S(2)}) collective-permute-start(bf16[128,2176]{1,0:T(8,128)(2,1)S(1)} %pad_maximum_fusion.refs_5_.refs_10_.refs_0_), channel_id=1, source_target_pairs={{0,32},{4,36},{8,40},{12,44},{16,48},{20,52},{24,56},{28,60},{32,0... | collective-permute-start | bytes 1671176 | tf_op jit(solution)/shard_map/ppermute | solution.py:28
  52.6 4.4 %collective-permute-done.21 = bf16[64,2176]{1,0:T(8,128)(2,1)S(1)} collective-permute-done((bf16[64,2176]{1,0:T(8,128)(2,1)S(1)}, bf16[64,2176]{1,0:T(8,128)(2,1)S(1)}, u32[]{:S(2)}, u32[]{:S(2)}) %collective-permute-start.21) | collective-permute-done | bytes 278560 | tf_op jit(solution)/shard_map/ppermute | solution.py:28
  57.0 2.6 %collective-permute-start.7 = (bf16[64,2048]{1,0:T(8,128)(2,1)S(1)}, bf16[64,2048]{1,0:T(8,128)(2,1)S(1)}, u32[]{:S(2)}, u32[]{:S(2)}) collective-permute-start(bf16[64,2048]{1,0:T(8,128)(2,1)S(1)} %slice.40), channel_id=1, source_target_pairs={{0,3},{1,2},{2,1},{3,0},{4,7},{5,6},{6,5},{7,4},{8,11},{9,10},{10,... | collective-permute-start | bytes 786440 | tf_op jit(solution)/shard_map/ppermute | solution.py:28
  59.8 4.7 %collective-permute-done.7.refs_3_ = bf16[64,2048]{1,0:T(8,128)(2,1)S(1)} collective-permute-done((bf16[64,2048]{1,0:T(8,128)(2,1)S(1)}, bf16[64,2048]{1,0:T(8,128)(2,1)S(1)}, u32[]{:S(2)}, u32[]{:S(2)}) %collective-permute-start.7) | collective-permute-done | bytes 262176 | tf_op jit(solution)/shard_map/ppermute | solution.py:28
  66.7 2.6 %collective-permute-done.11.refs_7_.refs_12_.refs_2_ = bf16[128,2176]{1,0:T(8,128)(2,1)S(1)} collective-permute-done((bf16[128,2176]{1,0:T(8,128)(2,1)S(1)}, bf16[128,2176]{1,0:T(8,128)(2,1)S(1)}, u32[]{:S(2)}, u32[]{:S(2)}) %collective-permute-start.11) | collective-permute-done | bytes 557088 | tf_op jit(solution)/shard_map/ppermute | solution.py:28
  72.4 7.4 %collective-permute-done.22.refs_16_.refs_5_ = bf16[128,2176]{1,0:T(8,128)(2,1)S(1)} collective-permute-done((bf16[128,2176]{1,0:T(8,128)(2,1)S(1)}, bf16[128,2176]{1,0:T(8,128)(2,1)S(1)}, u32[]{:S(2)}, u32[]{:S(2)}) %collective-permute-start.22) | collective-permute-done | bytes 557088 | tf_op jit(solution)/shard_map/ppermute | solution.py:28
  80.6 3.5 %collective-permute-start.12 = (bf16[128,1408]{1,0:T(8,128)(2,1)S(1)}, bf16[128,1408]{1,0:T(8,128)(2,1)S(1)}, u32[]{:S(2)}, u32[]{:S(2)}) collective-permute-start(bf16[128,1408]{1,0:T(8,128)(2,1)S(1)} %slice.42), channel_id=1, source_target_pairs={{0,96},{4,100},{8,104},{12,108},{16,112},{20,116},{24,120},{28,124... | collective-permute-start | bytes 1081352 | tf_op jit(solution)/shard_map/ppermute | solution.py:28
  84.0 3.3 %collective-permute-done.27.refs_15_.refs_4_ = bf16[128,2176]{1,0:T(8,128)(2,1)S(1)} collective-permute-done((bf16[128,2176]{1,0:T(8,128)(2,1)S(1)}, bf16[128,2176]{1,0:T(8,128)(2,1)S(1)}, u32[]{:S(2)}, u32[]{:S(2)}) %collective-permute-start.27) | collective-permute-done | bytes 557088 | tf_op jit(solution)/shard_map/ppermute | solution.py:28
  90.9 3.2 %collective-permute-start.38 = (bf16[128,768]{1,0:T(8,128)(2,1)S(1)}, bf16[128,768]{1,0:T(8,128)(2,1)S(1)}, u32[]{:S(2)}, u32[]{:S(2)}) collective-permute-start(bf16[128,768]{1,0:T(8,128)(2,1)S(1)} %slice.46), channel_id=1, source_target_pairs={{0,96},{4,100},{8,104},{12,108},{16,112},{20,116},{24,120},{28,124... | collective-permute-start | bytes 589832 | tf_op jit(solution)/shard_map/ppermute | solution.py:28
  98.1 2.6 %shard_map.123.refs_9_ = f32[512,1408]{1,0:T(8,128)S(1)} custom-call(bf16[128,2048]{1,0:T(8,128)(2,1)S(1)} %collective-permute-done.28.refs_0_, bf16[128,2048]{1,0:T(8,128)(2,1)S(1)} %collective-permute-done.29.refs_1_, bf16[128,2048]{1,0:T(8,128)(2,1)S(1)} %collective-permute-done.30.refs_2_, bf16[64,2048]{1,0:T(8,128)(2,1)S(1)} %collective-permute-done.31.refs_3_, ...), custom_call_target="tpu_custom_call" | custom-call | flops 2214592512 | bytes 10000000 | tf_op jit(solution)/shard_map/pallas_call | solution.py:37
  105.6 2.6 %shard_map.121.refs_9_ = f32[512,1408]{1,0:T(8,128)S(1)} custom-call(bf16[128,2048]{1,0:T(8,128)(2,1)S(1)} %shard_map.120.refs_0_.normed, bf16[128,2048]{1,0:T(8,128)(2,1)S(1)} %collective-permute-done.5.refs_1_, bf16[128,2048]{1,0:T(8,128)(2,1)S(1)} %collective-permute-done.6.refs_2_, bf16[64,2048]{1,0:T(8,128)(2,1)S(1)} %collective-permute-done.7.refs_3_, ...), custom_call_target="tpu_custom_call" | custom-call | flops 2214592512 | bytes 10000000 | tf_op jit(solution)/shard_map/pallas_call | solution.py:37
  110.7 2.6 %collective-permute-start.35 = (bf16[256,512]{1,0:T(8,128)(2,1)S(1)}, bf16[256,512]{1,0:T(8,128)(2,1)S(1)}, u32[]{:S(2)}, u32[]{:S(2)}) collective-permute-start(bf16[256,512]{1,0:T(8,128)(2,1)S(1)} %get-tuple-element.52), channel_id=1, source_target_pairs={{0,3},{1,2},{2,1},{3,0},{4,7},{5,6},{6,5},{7,4},{8,11},{9,10},{10,... | collective-permute-start | bytes 786440 | tf_op jit(solution)/shard_map/ppermute | solution.py:28
  116.3 3.4 %collective-permute-done.34.left = bf16[256,512]{1,0:T(8,128)(2,1)S(1)} collective-permute-done((bf16[256,512]{1,0:T(8,128)(2,1)S(1)}, bf16[256,512]{1,0:T(8,128)(2,1)S(1)}, u32[]{:S(2)}, u32[]{:S(2)}) %collective-permute-start.34) | collective-permute-done | bytes 262176 | tf_op jit(solution)/shard_map/ppermute | solution.py:28
  121.2 2.7 %collective-permute-start.36 = (bf16[128,512]{1,0:T(8,128)(2,1)S(1)}, bf16[128,512]{1,0:T(8,128)(2,1)S(1)}, u32[]{:S(2)}, u32[]{:S(2)}) collective-permute-start(bf16[128,512]{1,0:T(8,128)(2,1)S(1)} %get-tuple-element.56), channel_id=1, source_target_pairs={{0,3},{1,2},{2,1},{3,0},{4,7},{5,6},{6,5},{7,4},{8,11},{9,10},{10,... | collective-permute-start | bytes 393224 | tf_op jit(solution)/shard_map/ppermute | solution.py:28
  126.8 2.7 %collective-permute-start.45 = (bf16[128,512]{1,0:T(8,128)(2,1)S(1)}, bf16[128,512]{1,0:T(8,128)(2,1)S(1)}, u32[]{:S(2)}, u32[]{:S(2)}) collective-permute-start(bf16[128,512]{1,0:T(8,128)(2,1)S(1)} %get-tuple-element.65), channel_id=1, source_target_pairs={{0,3},{1,2},{2,1},{3,0},{4,7},{5,6},{6,5},{7,4},{8,11},{9,10},{10,... | collective-permute-start | bytes 393224 | tf_op jit(solution)/shard_map/ppermute | solution.py:28
  129.5 3.5 %collective-permute-done.45.refs_4_ = bf16[128,512]{1,0:T(8,128)(2,1)S(1)} collective-permute-done((bf16[128,512]{1,0:T(8,128)(2,1)S(1)}, bf16[128,512]{1,0:T(8,128)(2,1)S(1)}, u32[]{:S(2)}, u32[]{:S(2)}) %collective-permute-start.45) | collective-permute-done | bytes 131104 | tf_op jit(solution)/shard_map/ppermute | solution.py:28
  (108 shorter events, 48.7 us)
Async XLA Ops:
  3.1 23.4 %collective-permute-start.10 = (bf16[64,2176]{1,0:T(8,128)(2,1)S(1)}, bf16[64,2176]{1,0:T(8,128)(2,1)S(1)}, u32[]{:S(2)}, u32[]{:S(2)}) collective-permute-start(bf16[64,2176]{1,0:T(8,128)(2,1)S(1)} %get-tuple-element.68), channel_id=1, source_target_pairs={{0,8},{4,12},{8,0},{12,4},{16,24},{20,28},{24,16},{28,20},{32,40},... | collective-permute-start | bytes 835592 | tf_op jit(solution)/shard_map/ppermute | solution.py:28
  20.3 29.6 %collective-permute-start.5 = (bf16[128,2048]{1,0:T(8,128)(2,1)S(1)}, bf16[128,2048]{1,0:T(8,128)(2,1)S(1)}, u32[]{:S(2)}, u32[]{:S(2)}) collective-permute-start(bf16[128,2048]{1,0:T(8,128)(2,1)S(1)} %shard_map.120.refs_0_.normed), channel_id=1, source_target_pairs={{0,1},{1,0},{2,3},{3,2},{4,5},{5,4},{6,7},{7,6},{8,9},{9,8},{10,11... | collective-permute-start | bytes 1572872 | tf_op jit(solution)/shard_map/ppermute | solution.py:28
  21.0 29.3 %collective-permute-start.6 = (bf16[128,2048]{1,0:T(8,128)(2,1)S(1)}, bf16[128,2048]{1,0:T(8,128)(2,1)S(1)}, u32[]{:S(2)}, u32[]{:S(2)}) collective-permute-start(bf16[128,2048]{1,0:T(8,128)(2,1)S(1)} %shard_map.120.refs_0_.normed), channel_id=1, source_target_pairs={{0,3},{1,2},{2,1},{3,0},{4,7},{5,6},{6,5},{7,4},{8,11},{9,10},{10,... | collective-permute-start | bytes 1572872 | tf_op jit(solution)/shard_map/ppermute | solution.py:28
  21.6 38.0 %collective-permute-start.28 = (bf16[128,2048]{1,0:T(8,128)(2,1)S(1)}, bf16[128,2048]{1,0:T(8,128)(2,1)S(1)}, u32[]{:S(2)}, u32[]{:S(2)}) collective-permute-start(bf16[128,2048]{1,0:T(8,128)(2,1)S(1)} %shard_map.120.refs_0_.normed), channel_id=1, source_target_pairs={{0,4},{4,0},{8,12},{12,8},{16,20},{20,16},{24,28},{28,24},{32,36},... | collective-permute-start | bytes 1572872 | tf_op jit(solution)/shard_map/ppermute | solution.py:28
  21.6 14.1 %collective-permute-start.13 = (bf16[64,2176]{1,0:T(8,128)(2,1)S(1)}, bf16[64,2176]{1,0:T(8,128)(2,1)S(1)}, u32[]{:S(2)}, u32[]{:S(2)}) collective-permute-start(bf16[64,2176]{1,0:T(8,128)(2,1)S(1)} %get-tuple-element.68), channel_id=1, source_target_pairs={{0,24},{4,28},{8,16},{12,20},{16,8},{20,12},{24,0},{28,4},{32,56},... | collective-permute-start | bytes 835592 | tf_op jit(solution)/shard_map/ppermute | solution.py:28
  35.1 12.4 %collective-permute-start.14 = (bf16[64,2176]{1,0:T(8,128)(2,1)S(1)}, bf16[64,2176]{1,0:T(8,128)(2,1)S(1)}, u32[]{:S(2)}, u32[]{:S(2)}) collective-permute-start(bf16[64,2176]{1,0:T(8,128)(2,1)S(1)} %get-tuple-element.68), channel_id=1, source_target_pairs={{0,16},{4,20},{8,24},{12,28},{16,0},{20,4},{24,8},{28,12},{32,48},... | collective-permute-start | bytes 835592 | tf_op jit(solution)/shard_map/ppermute | solution.py:28
  35.7 10.2 %collective-permute-start.20 = (bf16[64,2176]{1,0:T(8,128)(2,1)S(1)}, bf16[64,2176]{1,0:T(8,128)(2,1)S(1)}, u32[]{:S(2)}, u32[]{:S(2)}) collective-permute-start(bf16[64,2176]{1,0:T(8,128)(2,1)S(1)} %get-tuple-element.67), channel_id=1, source_target_pairs={{0,96},{4,100},{8,104},{12,108},{16,112},{20,116},{24,120},{28,124... | collective-permute-start | bytes 835592 | tf_op jit(solution)/shard_map/ppermute | solution.py:28
  45.9 11.0 %collective-permute-start.21 = (bf16[64,2176]{1,0:T(8,128)(2,1)S(1)}, bf16[64,2176]{1,0:T(8,128)(2,1)S(1)}, u32[]{:S(2)}, u32[]{:S(2)}) collective-permute-start(bf16[64,2176]{1,0:T(8,128)(2,1)S(1)} %get-tuple-element.67), channel_id=1, source_target_pairs={{0,64},{4,68},{8,72},{12,76},{16,80},{20,84},{24,88},{28,92},{32,9... | collective-permute-start | bytes 835592 | tf_op jit(solution)/shard_map/ppermute | solution.py:28
  47.5 21.7 %collective-permute-start.11 = (bf16[128,2176]{1,0:T(8,128)(2,1)S(1)}, bf16[128,2176]{1,0:T(8,128)(2,1)S(1)}, u32[]{:S(2)}, u32[]{:S(2)}) collective-permute-start(bf16[128,2176]{1,0:T(8,128)(2,1)S(1)} %pad_maximum_fusion.refs_5_.refs_10_.refs_0_), channel_id=1, source_target_pairs={{0,32},{4,36},{8,40},{12,44},{16,48},{20,52},{24,56},{28,60},{32,0... | collective-permute-start | bytes 1671176 | tf_op jit(solution)/shard_map/ppermute | solution.py:28
  49.9 19.5 %collective-permute-start.15 = (bf16[128,2176]{1,0:T(8,128)(2,1)S(1)}, bf16[128,2176]{1,0:T(8,128)(2,1)S(1)}, u32[]{:S(2)}, u32[]{:S(2)}) collective-permute-start(bf16[128,2176]{1,0:T(8,128)(2,1)S(1)} %constant_dynamic-update-slice_fusion.refs_6_.refs_11_.refs_1_), channel_id=1, source_target_pairs={{0,96},{4,100},{8,104},{12,108},{16,112},{20,116},{24,120},{28,124... | collective-permute-start | bytes 1671176 | tf_op jit(solution)/shard_map/ppermute | solution.py:28
  50.3 21.1 %collective-permute-start.18 = (bf16[128,2176]{1,0:T(8,128)(2,1)S(1)}, bf16[128,2176]{1,0:T(8,128)(2,1)S(1)}, u32[]{:S(2)}, u32[]{:S(2)}) collective-permute-start(bf16[128,2176]{1,0:T(8,128)(2,1)S(1)} %pad_maximum_fusion.1.refs_11_.refs_14_.refs_4_), channel_id=1, source_target_pairs={{0,8},{4,12},{8,0},{12,4},{16,24},{20,28},{24,16},{28,20},{32,40},... | collective-permute-start | bytes 1671176 | tf_op jit(solution)/shard_map/ppermute | solution.py:28
  64.5 15.3 %collective-permute-start.22 = (bf16[128,2176]{1,0:T(8,128)(2,1)S(1)}, bf16[128,2176]{1,0:T(8,128)(2,1)S(1)}, u32[]{:S(2)}, u32[]{:S(2)}) collective-permute-start(bf16[128,2176]{1,0:T(8,128)(2,1)S(1)} %constant_dynamic-update-slice_fusion.2.refs_12_.refs_15_.refs_5_), channel_id=1, source_target_pairs={{0,24},{4,28},{8,16},{12,20},{16,8},{20,12},{24,0},{28,4},{32,56},... | collective-permute-start | bytes 1671176 | tf_op jit(solution)/shard_map/ppermute | solution.py:28
  66.3 13.5 %collective-permute-start.24 = (bf16[128,2176]{1,0:T(8,128)(2,1)S(1)}, bf16[128,2176]{1,0:T(8,128)(2,1)S(1)}, u32[]{:S(2)}, u32[]{:S(2)}) collective-permute-start(bf16[128,2176]{1,0:T(8,128)(2,1)S(1)} %constant_dynamic-update-slice_fusion.refs_6_.refs_11_.refs_1_), channel_id=1, source_target_pairs={{0,32},{4,36},{8,40},{12,44},{16,48},{20,52},{24,56},{28,60},{32,0... | collective-permute-start | bytes 1671176 | tf_op jit(solution)/shard_map/ppermute | solution.py:28
  69.2 11.2 %collective-permute-start.25 = (bf16[128,2176]{1,0:T(8,128)(2,1)S(1)}, bf16[128,2176]{1,0:T(8,128)(2,1)S(1)}, u32[]{:S(2)}, u32[]{:S(2)}) collective-permute-start(bf16[128,2176]{1,0:T(8,128)(2,1)S(1)} %pad_maximum_fusion.refs_5_.refs_10_.refs_0_), channel_id=1, source_target_pairs={{0,96},{4,100},{8,104},{12,108},{16,112},{20,116},{24,120},{28,124... | collective-permute-start | bytes 1671176 | tf_op jit(solution)/shard_map/ppermute | solution.py:28
  69.4 11.2 %collective-permute-start.26 = (bf16[128,2176]{1,0:T(8,128)(2,1)S(1)}, bf16[128,2176]{1,0:T(8,128)(2,1)S(1)}, u32[]{:S(2)}, u32[]{:S(2)}) collective-permute-start(bf16[128,2176]{1,0:T(8,128)(2,1)S(1)} %constant_dynamic-update-slice_fusion.2.refs_12_.refs_15_.refs_5_), channel_id=1, source_target_pairs={{0,8},{4,12},{8,0},{12,4},{16,24},{20,28},{24,16},{28,20},{32,40},... | collective-permute-start | bytes 1671176 | tf_op jit(solution)/shard_map/ppermute | solution.py:28
  71.4 16.0 %collective-permute-start.27 = (bf16[128,2176]{1,0:T(8,128)(2,1)S(1)}, bf16[128,2176]{1,0:T(8,128)(2,1)S(1)}, u32[]{:S(2)}, u32[]{:S(2)}) collective-permute-start(bf16[128,2176]{1,0:T(8,128)(2,1)S(1)} %pad_maximum_fusion.1.refs_11_.refs_14_.refs_4_), channel_id=1, source_target_pairs={{0,24},{4,28},{8,16},{12,20},{16,8},{20,12},{24,0},{28,4},{32,56},... | collective-permute-start | bytes 1671176 | tf_op jit(solution)/shard_map/ppermute | solution.py:28
  79.8 9.5 %collective-permute-start.30 = (bf16[128,2048]{1,0:T(8,128)(2,1)S(1)}, bf16[128,2048]{1,0:T(8,128)(2,1)S(1)}, u32[]{:S(2)}, u32[]{:S(2)}) collective-permute-start(bf16[128,2048]{1,0:T(8,128)(2,1)S(1)} %collective-permute-done.6.refs_2_), channel_id=1, source_target_pairs={{0,4},{4,0},{8,12},{12,8},{16,20},{20,16},{24,28},{28,24},{32,36},... | collective-permute-start | bytes 1572872 | tf_op jit(solution)/shard_map/ppermute | solution.py:28
  80.6 13.5 %collective-permute-start.12 = (bf16[128,1408]{1,0:T(8,128)(2,1)S(1)}, bf16[128,1408]{1,0:T(8,128)(2,1)S(1)}, u32[]{:S(2)}, u32[]{:S(2)}) collective-permute-start(bf16[128,1408]{1,0:T(8,128)(2,1)S(1)} %slice.42), channel_id=1, source_target_pairs={{0,96},{4,100},{8,104},{12,108},{16,112},{20,116},{24,120},{28,124... | collective-permute-start | bytes 1081352 | tf_op jit(solution)/shard_map/ppermute | solution.py:28
  87.5 9.9 %collective-permute-start.19 = (bf16[128,1408]{1,0:T(8,128)(2,1)S(1)}, bf16[128,1408]{1,0:T(8,128)(2,1)S(1)}, u32[]{:S(2)}, u32[]{:S(2)}) collective-permute-start(bf16[128,1408]{1,0:T(8,128)(2,1)S(1)} %slice.44), channel_id=1, source_target_pairs={{0,24},{4,28},{8,16},{12,20},{16,8},{20,12},{24,0},{28,4},{32,56},... | collective-permute-start | bytes 1081352 | tf_op jit(solution)/shard_map/ppermute | solution.py:28
  89.4 11.4 %collective-permute-start.23 = (bf16[128,1408]{1,0:T(8,128)(2,1)S(1)}, bf16[128,1408]{1,0:T(8,128)(2,1)S(1)}, u32[]{:S(2)}, u32[]{:S(2)}) collective-permute-start(bf16[128,1408]{1,0:T(8,128)(2,1)S(1)} %slice.45), channel_id=1, source_target_pairs={{0,8},{4,12},{8,0},{12,4},{16,24},{20,28},{24,16},{28,20},{32,40},... | collective-permute-start | bytes 1081352 | tf_op jit(solution)/shard_map/ppermute | solution.py:28
  90.9 11.8 %collective-permute-start.38 = (bf16[128,768]{1,0:T(8,128)(2,1)S(1)}, bf16[128,768]{1,0:T(8,128)(2,1)S(1)}, u32[]{:S(2)}, u32[]{:S(2)}) collective-permute-start(bf16[128,768]{1,0:T(8,128)(2,1)S(1)} %slice.46), channel_id=1, source_target_pairs={{0,96},{4,100},{8,104},{12,108},{16,112},{20,116},{24,120},{28,124... | collective-permute-start | bytes 589832 | tf_op jit(solution)/shard_map/ppermute | solution.py:28
  110.7 10.4 %collective-permute-start.35 = (bf16[256,512]{1,0:T(8,128)(2,1)S(1)}, bf16[256,512]{1,0:T(8,128)(2,1)S(1)}, u32[]{:S(2)}, u32[]{:S(2)}) collective-permute-start(bf16[256,512]{1,0:T(8,128)(2,1)S(1)} %get-tuple-element.52), channel_id=1, source_target_pairs={{0,3},{1,2},{2,1},{3,0},{4,7},{5,6},{6,5},{7,4},{8,11},{9,10},{10,... | collective-permute-start | bytes 786440 | tf_op jit(solution)/shard_map/ppermute | solution.py:28
  114.3 10.6 %collective-permute-start.43 = (bf16[256,512]{1,0:T(8,128)(2,1)S(1)}, bf16[256,512]{1,0:T(8,128)(2,1)S(1)}, u32[]{:S(2)}, u32[]{:S(2)}) collective-permute-start(bf16[256,512]{1,0:T(8,128)(2,1)S(1)} %get-tuple-element.60), channel_id=1, source_target_pairs={{0,1},{1,0},{2,3},{3,2},{4,5},{5,4},{6,7},{7,6},{8,9},{9,8},{10,11... | collective-permute-start | bytes 786440 | tf_op jit(solution)/shard_map/ppermute | solution.py:28
  115.7 11.0 %collective-permute-start.44 = (bf16[256,512]{1,0:T(8,128)(2,1)S(1)}, bf16[256,512]{1,0:T(8,128)(2,1)S(1)}, u32[]{:S(2)}, u32[]{:S(2)}) collective-permute-start(bf16[256,512]{1,0:T(8,128)(2,1)S(1)} %get-tuple-element.61), channel_id=1, source_target_pairs={{0,3},{1,2},{2,1},{3,0},{4,7},{5,6},{6,5},{7,4},{8,11},{9,10},{10,... | collective-permute-start | bytes 786440 | tf_op jit(solution)/shard_map/ppermute | solution.py:28
  (27 other events, 199.6 us)
